TPU v7x, 32 devices: a whole 2x2x4 slice. The times are simulated.
32 devices in a mesh: sp: 8 (over z, y), tp: 4 (over x, core).
Axes of the slice: x: 2, y: 2, z: 4, core: 2. Of those that a mesh axis runs over, the one named last changes fastest.
Arguments:
- cotangent: bfloat16 [1280, 2048], P('sp'), may hold values from -8 to 8
- saved_input: bfloat16 [1280, 2048], P('sp'), may hold values from -200 to 200
- routes: int32 [1280, 2], P('sp'), may hold values from 0 to 7, all different within a row; in each aligned block of 160 rows (0 to 159, 160 to 319, ...) at most 80 rows name the same one
- route_weight: float32 [1280, 2], P('sp'), may hold values from 0.2 to 1.5
- gate_proj: bfloat16 [8, 2048, 1024], P('sp', None, 'tp'), may hold values from -0.125 to 0.125
- up_proj: bfloat16 [8, 2048, 1024], P('sp', None, 'tp'), may hold values from -0.125 to 0.125
- down_proj: bfloat16 [8, 1024, 2048], P('sp', 'tp'), may hold values from -0.1875 to 0.1875
- out_proj: bfloat16 [2048, 1024], P(None, 'tp'), may hold values from -0.1875 to 0.1875
- conv_input: bfloat16 [1280, 1024], P('sp', 'tp'), may hold values from -6 to 6
- gate_branch: bfloat16 [1280, 1024], P('sp', 'tp'), may hold values from -6 to 6
- conv_taps: bfloat16 [4, 1024], P(None, 'tp'), may hold values from -3 to 3
- recur_map: bfloat16 [2, 16, 64, 64], P(None, 'tp'), may hold values from -0.75 to 0.75
- input_map: bfloat16 [2, 16, 64, 64], P(None, 'tp'), may hold values from -0.75 to 0.75
- decay_param: float32 [2, 1024], P(None, 'tp'), may hold values from 4 to 30
- decay_shift: float32 [2, 1280, 1024], P(None, 'sp', 'tp'), may hold values from -2 to 0, as said below
Outputs:
- grad_gate_proj: float32 [8, 2048, 1024], P('sp', None, 'tp')
- grad_up_proj: float32 [8, 2048, 1024], P('sp', None, 'tp')
- grad_down_proj: float32 [8, 1024, 2048], P('sp', 'tp')
- grad_out_proj: float32 [2048, 1024], P('sp', 'tp')
- grad_conv_input: bfloat16 [1280, 1024], P('sp', 'tp')
- grad_gate_branch: bfloat16 [1280, 1024], P('sp', 'tp')
Inputs may be any that keep to these rules, and one draw needn't show every extreme that they name: Each row names 2 different experts; among the rows of one device no expert is named by more than 80 rows, and in every draw some device routes exactly 80 rows to some expert. `decay_shift`: together with decay_param, -log_decay stays at or above softplus(-decay_param) for every channel and position.
All inputs are finite; a program needn't handle non-finite values.
Results may differ from a plain program's by a relative error of at most 0.013.
Values may be sent and summed in bfloat16 or wider, within the bound.
A program may use at most 128 MiB of HBM per device.

v0:
```python
import functools
import jax
import jax.numpy as jnp
from jax import lax
from jax.experimental import pallas as pl
from jax.experimental.pallas import tpu as pltpu
from jax.sharding import PartitionSpec as P

EPS = 1e-06
DECAY_SCALE = 8.0
ROW_TILE = 16
GELU_K = 0.7978845608028654
GELU_C = 0.044715
VM = pl.BlockSpec(memory_space=pltpu.VMEM)
BF = jnp.bfloat16
F32 = jnp.float32


def local_call(kernel, args, outs, cost=10_000_000):
    return pl.pallas_call(
        kernel,
        out_shape=outs,
        in_specs=[VM] * len(args),
        out_specs=jax.tree.map(lambda _: VM, outs),
        compiler_params=pltpu.CompilerParams(vmem_limit_bytes=56 * 2**20),
        cost_estimate=pl.CostEstimate(flops=cost, bytes_accessed=4_000_000, transcendentals=0),
    )(*args)


def prepare_kernel(slots, cot_ref, x_ref, routes_ref, weight_ref, sends_ref, sendi_ref, pick_ref):
    length, width = cot_ref.shape
    experts = sends_ref.shape[0]
    fourth = sends_ref.shape[2]
    tp = lax.axis_index("tp")
    cols = pl.ds(pl.multiple_of(tp * fourth, 128), fourth)
    x = x_ref[...].astype(F32)
    inv = lax.rsqrt(jnp.mean(x * x, axis=1, keepdims=True) + EPS)
    mine = (x_ref[:, cols].astype(F32) * inv).astype(BF)
    routes = routes_ref[...]
    weight = weight_ref[...]
    which = lax.broadcasted_iota(jnp.int32, (experts, length), 0)
    first = which == routes[0:1]
    second = which == routes[1:2]
    named = (first | second).astype(F32).astype(BF)
    earlier = lax.broadcasted_iota(jnp.int32, (length, length), 0) < lax.broadcasted_iota(
        jnp.int32, (length, length), 1
    )
    rank = jnp.dot(named, earlier.astype(F32).astype(BF), preferred_element_type=F32)
    place = which * slots + rank.astype(jnp.int32)
    target0 = jnp.sum(jnp.where(first, place, 0).astype(F32), axis=0, keepdims=True).astype(jnp.int32)
    target1 = jnp.sum(jnp.where(second, place, 0).astype(F32), axis=0, keepdims=True).astype(jnp.int32)
    slot = lax.broadcasted_iota(jnp.int32, (experts * slots, length), 0)
    hit0 = slot == target0
    hit1 = slot == target1
    pick = (hit0 | hit1).astype(F32).astype(BF)
    pick_ref[...] = pick
    share = jnp.where(hit0, weight[0:1], 0.0) + jnp.where(hit1, weight[1:2], 0.0)
    share = jnp.sum(share, axis=1, keepdims=True)
    got = jnp.dot(pick, mine, preferred_element_type=F32).astype(BF)
    sendi_ref[...] = got.reshape(experts, slots, fourth)
    cot = jnp.dot(pick, cot_ref[:, cols], preferred_element_type=F32)
    sends_ref[...] = (cot * share).astype(BF).reshape(experts, slots, fourth)


def neighbours():
    tp = lax.axis_index("tp")
    side = tp // 2
    core = tp % 2
    return tp, side * 2 + (1 - core), (1 - side) * 2 + core, (1 - side) * 2 + (1 - core)


def greet(n, with_sp=True, with_tp=True):
    sp = lax.axis_index("sp")
    tp, partner, across, _ = neighbours()
    barrier = pltpu.get_barrier_semaphore()
    count = 0
    if with_sp:
        for d in range(1, n):
            pl.semaphore_signal(
                barrier, inc=1, device_id=((sp + d) % n, tp), device_id_type=pl.DeviceIdType.MESH
            )
        count += n - 1
    if with_tp:
        for other in (partner, across):
            pl.semaphore_signal(
                barrier, inc=1, device_id=(sp, other), device_id_type=pl.DeviceIdType.MESH
            )
        count += 2
    pl.semaphore_wait(barrier, count)


def partner_at(sp, n, d):
    if n & (n - 1):
        return (sp + d) % n
    bit, peer = 1, sp
    while bit < n:
        if d & bit:
            peer = peer + bit * (1 - 2 * ((sp // bit) % 2))
        bit *= 2
    return peer


def source_at(sp, n, d):
    return (sp + n - d) % n if n & (n - 1) else partner_at(sp, n, d)


def edge_copies(n, x_ref, halo_ref, sems):
    sp = lax.axis_index("sp")
    tp = lax.axis_index("tp")
    length, tile = x_ref.shape[0], halo_ref.shape[1]
    copies = (
        remote(x_ref.at[pl.ds(length - tile, tile)], halo_ref.at[0], sems, (0,), ((sp + 1) % n, tp)),
        remote(x_ref.at[pl.ds(0, tile)], halo_ref.at[1], sems, (1,), ((sp + n - 1) % n, tp)),
    )
    for copy in copies:
        copy.start()
    return copies


def halo_edges(halo, n, width):
    sp = lax.axis_index("sp")
    zero = jnp.zeros((), halo.dtype)
    return (
        jnp.where(sp == 0, zero, halo[0, halo.shape[1] - width :]),
        jnp.where(sp == n - 1, zero, halo[1, :width]),
    )


def remote(src, dst, sems, index, device):
    return pltpu.make_async_remote_copy(
        src_ref=src,
        dst_ref=dst,
        send_sem=sems.at[(0,) + index],
        recv_sem=sems.at[(1,) + index],
        device_id=device,
        device_id_type=pl.DeviceIdType.MESH,
    )


def dispatch_kernel(
    n, sends_ref, sendi_ref, x_ref, outs_ref, outi_ref, halo_ref, hop, pair, cross, fwd, own, edge
):
    fourth = sends_ref.shape[2]
    sp = lax.axis_index("sp")
    tp, partner, across, _ = neighbours()

    def cols(q):
        return pl.ds(pl.multiple_of(q * fourth, 128), fourth)

    mine, theirs = cols(tp), cols(across)
    arrays = ((sends_ref, outs_ref), (sendi_ref, outi_ref))
    greet(n)
    hops = {}
    pending = list(edge_copies(n, x_ref, halo_ref, edge))
    away = [1] + [d for p in (0, 1) for d in range(n - 1, 1, -1) if d % 2 == p]
    for a, (src, dst) in enumerate(arrays):
        local = pltpu.make_async_copy(src.at[sp], dst.at[sp, :, mine], own.at[a])
        local.start()
        hops[a, 0] = local
    for d in away:
        peer = partner_at(sp, n, d)
        for a, (src, dst) in enumerate(arrays):
            copy = remote(src.at[peer], dst.at[sp, :, mine], hop, (a, d), (peer, tp))
            copy.start()
            hops[a, d] = copy

    def step_in(a, d):
        dst = arrays[a][1]
        source = source_at(sp, n, d)
        if d == 0:
            hops[a, d].wait()
        else:
            hops[a, d].wait_recv()
        block = dst.at[source, :, mine]
        over = remote(block, block, cross, (a, d), (sp, across))
        over.start()
        near = remote(block, block, pair, (a, d), (sp, partner))
        near.start()
        pending.append(near)
        return over

    def step_on(a, d, over):
        dst = arrays[a][1]
        source = source_at(sp, n, d)
        over.wait_recv()
        block = dst.at[source, :, theirs]
        copy = remote(block, block, fwd, (a, d), (sp, partner))
        copy.start()
        pending.append(copy)

    order = [(a, d) for d in [0] + away for a in range(2)]
    overs = []
    lag = 2
    for i, (a, d) in enumerate(order):
        overs.append(step_in(a, d))
        if i >= lag:
            step_on(*order[i - lag], overs[i - lag])
    for i in range(max(len(order) - lag, 0), len(order)):
        step_on(*order[i], overs[i])
    for copy in pending:
        copy.wait()
    for over in overs:
        over.wait_send()
    for d in range(1, n):
        for a in range(2):
            hops[a, d].wait_send()


def dispatch(sends, sendi, x, n, n_tp):
    experts, slots, fourth = sends.shape
    full = jax.ShapeDtypeStruct((experts, slots, fourth * n_tp), BF)
    dma = pltpu.SemaphoreType.DMA
    return pl.pallas_call(
        functools.partial(dispatch_kernel, n),
        out_shape=(full, full, jax.ShapeDtypeStruct((2, ROW_TILE, x.shape[1]), x.dtype)),
        in_specs=[VM, VM, VM],
        out_specs=(VM, VM, VM),
        scratch_shapes=[dma((2, 2, n))] * 4 + [dma((2,)), dma((2, 2))],
        compiler_params=pltpu.CompilerParams(
            collective_id=1, has_side_effects=True, vmem_limit_bytes=40 * 2**20
        ),
        cost_estimate=pl.CostEstimate(flops=0, bytes_accessed=100_000_000, transcendentals=0),
    )(sends, sendi, x)


def return_kernel(
    n, part_ref, pick_ref, out_ref, got1, got2, mid, fin, back, s_pair, s_cross, s_hop, s_tail
):
    fourth = got2.shape[2]
    slots = got2.shape[1]
    sp = lax.axis_index("sp")
    tp, partner, across, diagonal = neighbours()

    def cols(q):
        return pl.ds(pl.multiple_of(q * fourth, 128), fourth)

    greet(n)
    order = list(range(n - 1, -1, -1))
    pairs, crosses, hops = {}, {}, {}
    for d in order:
        j = partner_at(sp, n, d)
        for a, q in enumerate((diagonal, partner)):
            copy = remote(
                part_ref.at[j, :, cols(q)], got1.at[a, j], s_pair, (a, d), (sp, partner)
            )
            copy.start()
            pairs[a, d] = copy

    def stage_b(d):
        j = partner_at(sp, n, d)
        pairs[0, d].wait_recv()
        total = part_ref[j, :, cols(across)].astype(F32) + got1[0, j].astype(F32)
        mid[j] = total.astype(BF)
        copy = remote(mid.at[j], got2.at[j], s_cross, (d,), (sp, across))
        copy.start()
        crosses[d] = copy

    def stage_c(d):
        j = partner_at(sp, n, d)
        pairs[1, d].wait_recv()
        crosses[d].wait_recv()
        total = part_ref[j, :, cols(tp)].astype(F32) + got1[1, j].astype(F32)
        total = (total + got2[j].astype(F32)).astype(BF)
        if d == 0:
            back[sp] = total
        else:
            fin[j] = total
            copy = remote(fin.at[j], back.at[sp], s_hop, (d,), (j, tp))
            copy.start()
            hops[d] = copy

    lag = 2
    for i, d in enumerate(order):
        stage_b(d)
        if i >= lag:
            stage_c(order[i - lag])
    for d in order[max(n - lag, 0):]:
        stage_c(d)
    for d in range(1, n):
        hops[d].wait_recv()
    rows = back[...].reshape(n * slots, fourth)
    grad = lax.dot_general(
        pick_ref[...], rows, (((0,), (0,)), ((), ())), preferred_element_type=F32
    )
    out_ref[:, cols(tp)] = grad.astype(BF)
    own = out_ref.at[:, cols(tp)]
    over = remote(own, own, s_tail, (0,), (sp, across))
    near = remote(own, own, s_tail, (1,), (sp, partner))
    over.start()
    near.start()
    over.wait_recv()
    other = out_ref.at[:, cols(across)]
    last = remote(other, other, s_tail, (2,), (sp, partner))
    last.start()
    for d in range(n):
        for a in range(2):
            pairs[a, d].wait_send()
        crosses[d].wait_send()
        if d:
            hops[d].wait_send()
    near.wait()
    over.wait_send()
    last.wait()


def send_back(part, pick, n, n_tp):
    _, slots, width = part.shape
    fourth = width // n_tp
    dma = pltpu.SemaphoreType.DMA
    block = (n, slots, fourth)
    return pl.pallas_call(
        functools.partial(return_kernel, n),
        out_shape=jax.ShapeDtypeStruct((pick.shape[1], width), BF),
        in_specs=[VM, VM],
        out_specs=VM,
        scratch_shapes=[pltpu.VMEM((2,) + block, BF)]
        + [pltpu.VMEM(block, BF)] * 4
        + [dma((2, 2, n)), dma((2, n)), dma((2, n)), dma((2, 3))],
        compiler_params=pltpu.CompilerParams(
            collective_id=2, has_side_effects=True, vmem_limit_bytes=40 * 2**20
        ),
        cost_estimate=pl.CostEstimate(flops=0, bytes_accessed=100_000_000, transcendentals=0),
    )(part, pick)


def exchange_kernel(n, same, halo, *refs):
    if halo:
        src_ref, x_ref, dst_ref, halo_ref, sems, own, edge = refs
    else:
        src_ref, dst_ref, sems, own = refs
    sp = lax.axis_index("sp")
    tp = lax.axis_index("tp")

    def piece(i):
        return src_ref if same else src_ref.at[i]

    greet(n, with_tp=False)
    copies = list(edge_copies(n, x_ref, halo_ref, edge)) if halo else []
    local = pltpu.make_async_copy(piece(sp), dst_ref.at[sp], own.at[0])
    local.start()
    for d in range(n - 1, 0, -1):
        peer = partner_at(sp, n, d)
        copy = remote(piece(peer), dst_ref.at[sp], sems, (d,), (peer, tp))
        copy.start()
        copies.append(copy)
    local.wait()
    for copy in copies:
        copy.wait()


def exchange(x, n, same, cid, edges=None):
    out = [jax.ShapeDtypeStruct((n,) + x.shape if same else x.shape, x.dtype)]
    dma = pltpu.SemaphoreType.DMA
    scratch = [dma((2, n)), dma((1,))]
    args = [x]
    if edges is not None:
        args.append(edges)
        out.append(jax.ShapeDtypeStruct((2, ROW_TILE, edges.shape[1]), edges.dtype))
        scratch.append(dma((2, 2)))
    return pl.pallas_call(
        functools.partial(exchange_kernel, n, same, edges is not None),
        out_shape=out,
        in_specs=[VM] * len(args),
        out_specs=[VM] * len(out),
        scratch_shapes=scratch,
        compiler_params=pltpu.CompilerParams(
            collective_id=cid, has_side_effects=True, vmem_limit_bytes=24 * 2**20
        ),
        cost_estimate=pl.CostEstimate(flops=0, bytes_accessed=20_000_000, transcendentals=0),
    )(*args)


def split_dot(x, w, dims):
    high = x.astype(BF)
    rest = x - high.astype(F32)
    middle = rest.astype(BF)
    low = (rest - middle.astype(F32)).astype(BF)
    total = lax.dot_general(low, w, dims, preferred_element_type=F32)
    total = total + lax.dot_general(middle, w, dims, preferred_element_type=F32)
    return total + lax.dot_general(high, w, dims, preferred_element_type=F32)


def minus_expm1(y):
    series = 1.0 + y * (1.0 / 8.0)
    for k in (7.0, 6.0, 5.0, 4.0, 3.0, 2.0):
        series = 1.0 + y * (1.0 / k) * series
    return jnp.where(y > -0.25, -y * series, 1.0 - jnp.exp(y))


def shifted(x, by, edge):
    length = x.shape[0]
    row = lax.broadcasted_iota(jnp.int32, x.shape, 0)
    moved = pltpu.roll(x, by % length, 0)
    return jnp.where(row == (0 if by > 0 else length - 1), edge, moved)


def run_scans(length, jobs):
    width = jobs[0][1].shape[1]
    groups = length // 8

    def body(g, carry):
        out = []
        for (reverse, a_ref, b_ref, to_ref), state in zip(jobs, carry):
            base = pl.multiple_of((groups - 1 - g if reverse else g) * 8, 8)
            a = a_ref[pl.ds(base, 8), :]
            b = None if b_ref is None else b_ref[pl.ds(base, 8), :]
            rows = [None] * 8
            for k in reversed(range(8)) if reverse else range(8):
                state = a[k : k + 1] * state
                if b is not None:
                    state = state + b[k : k + 1]
                rows[k] = state
            to_ref[pl.ds(base, 8), :] = jnp.concatenate(rows, axis=0)
            out.append(state)
        return tuple(out)

    start = tuple(
        jnp.full((1, width), 1.0 if b_ref is None else 0.0, F32) for _, _, b_ref, _ in jobs
    )
    return lax.fori_loop(0, groups, body, start)


def pre_kernel(
    x_ref, low_ref, high_ref, taps_ref, maps_ref, plus_ref, shift_ref,
    conv_ref, gates_ref, decay_ref, root_ref, state_ref, cum_ref, after_ref, tot_ref, drive_ref,
):
    length, width = x_ref.shape
    taps = taps_ref[...].astype(F32)
    low = low_ref[...].astype(F32)
    high = high_ref[...].astype(F32)
    x = x_ref[...].astype(F32)
    back1 = shifted(x, 1, low[1:2])
    back2 = shifted(back1, 1, low[0:1])
    conv = back2 * taps[0:1] + back1 * taps[1:2] + x * taps[2:3]
    conv = conv + shifted(x, -1, high[0:1]) * taps[3:4]
    conv_ref[...] = conv
    gates = jax.nn.sigmoid(split_dot(conv, maps_ref[...], (((1,), (0,)), ((), ()))))
    gates_ref[...] = gates
    for d in range(2):
        recur = gates[:, 2 * d * width : (2 * d + 1) * width]
        inputs = gates[:, (2 * d + 1) * width : (2 * d + 2) * width]
        log_decay = -DECAY_SCALE * recur * plus_ref[d : d + 1, :] + shift_ref[d]
        root = jnp.sqrt(minus_expm1(2.0 * log_decay))
        decay_ref[d] = jnp.exp(log_decay)
        root_ref[d] = root
        drive_ref[d] = root * (inputs * conv)
    a_f, a_b = decay_ref.at[0], decay_ref.at[1]
    ends = run_scans(
        length,
        (
            (False, a_f, drive_ref.at[0], state_ref.at[0]),
            (True, a_b, drive_ref.at[1], state_ref.at[1]),
            (False, a_f, None, cum_ref.at[0]),
            (True, a_b, None, cum_ref.at[1]),
            (True, a_f, None, after_ref.at[0]),
            (False, a_b, None, after_ref.at[1]),
        ),
    )
    tot_ref[0:1, :] = ends[2]
    tot_ref[1:2, :] = ends[0]
    tot_ref[2:3, :] = ends[3]
    tot_ref[3:4, :] = ends[1]
    tot_ref[4:8, :] = jnp.zeros((4, width), F32)


def gelu_parts(x):
    t = jnp.tanh(GELU_K * (x + GELU_C * x * x * x))
    value = 0.5 * x * (1.0 + t)
    slope = 0.5 * (1.0 + t) + 0.5 * x * (1.0 - t * t) * GELU_K * (1.0 + 3.0 * GELU_C * x * x)
    return value, slope


def middle_kernel(
    ng_ref, cot_ref, x_ref, proj_ref, branch_ref, decay_ref, tot_ref,
    mixed_ref, out_grad_ref, carried_ref, after_ref, tot2_ref, drive_ref,
):
    length = ng_ref.shape[0]
    x = x_ref[...].astype(F32)
    inv = lax.rsqrt(jnp.mean(x * x, axis=1, keepdims=True) + EPS)
    normed = x * inv
    ng = ng_ref[...].astype(F32)
    dot = jnp.mean(ng * normed, axis=1, keepdims=True)
    mixed = (cot_ref[...].astype(F32) + inv * (ng - normed * dot)).astype(BF)
    mixed_ref[...] = mixed
    out_grad = jnp.dot(mixed, proj_ref[...], preferred_element_type=F32)
    out_grad_ref[...] = out_grad
    value, _ = gelu_parts(branch_ref[...].astype(F32))
    carried = out_grad * value
    carried_ref[...] = carried
    drive_ref[...] = decay_ref[...] * carried[None]
    ends = run_scans(
        length,
        (
            (True, decay_ref.at[0], drive_ref.at[0], after_ref.at[0]),
            (False, decay_ref.at[1], drive_ref.at[1], after_ref.at[1]),
        ),
    )
    tot2_ref[0:4, :] = tot_ref[0:4, :]
    tot2_ref[4:5, :] = ends[1]
    tot2_ref[5:6, :] = ends[0]
    tot2_ref[6:8, :] = jnp.zeros((2, tot_ref.shape[1]), F32)


def last_kernel(
    n, all_ref, conv_ref, gates_ref, decay_ref, root_ref, state_ref, cum_ref, ones_ref,
    after_ref, carried_ref, out_grad_ref, branch_ref, maps_ref, plus_ref,
    conv_grad_ref, branch_grad_ref, mixed_out_ref, packed_ref,
):
    length, width = conv_ref.shape
    sp = lax.axis_index("sp")
    zero = jnp.zeros((1, width), F32)

    def lower(k, carry):
        t = all_ref[k]
        return (t[0:1] * carry[0] + t[1:2], t[2:3] * carry[1] + t[4:5])

    def upper(i, carry):
        t = all_ref[n - 1 - i]
        return (t[2:3] * carry[0] + t[3:4], t[0:1] * carry[1] + t[5:6])

    in_f, in_ab = lax.fori_loop(0, sp, lower, (zero, zero))
    in_b, in_af = lax.fori_loop(0, n - 1 - sp, upper, (zero, zero))
    state_f = state_ref[0] + cum_ref[0] * in_f
    state_b = state_ref[1] + cum_ref[1] * in_b
    after_f = after_ref[0] + ones_ref[0] * in_af
    after_b = after_ref[1] + ones_ref[1] * in_ab
    carried = carried_ref[...]
    adjoint = (carried + shifted(after_f, -1, in_af), carried + shifted(after_b, 1, in_ab))
    beside = (shifted(state_f, 1, in_f), shifted(state_b, -1, in_b))
    conv = conv_ref[...]
    total = jnp.zeros((length, width), F32)
    for d in range(2):
        recur = gates_ref[:, 2 * d * width : (2 * d + 1) * width]
        inputs = gates_ref[:, (2 * d + 1) * width : (2 * d + 2) * width]
        decay = decay_ref[d]
        root = root_ref[d]
        g = adjoint[d]
        total = total + g * root * inputs
        g_log = g * beside[d] * decay - g * inputs * conv * (decay * decay) / root
        g_recur = g_log * (-DECAY_SCALE * plus_ref[d : d + 1, :])
        packed_ref[:, 2 * d * width : (2 * d + 1) * width] = g_recur * recur * (1.0 - recur)
        packed_ref[:, (2 * d + 1) * width : (2 * d + 2) * width] = (
            g * root * conv * inputs * (1.0 - inputs)
        )
    total = total + split_dot(packed_ref[...], maps_ref[...], (((1,), (1,)), ((), ())))
    conv_grad_ref[...] = total.astype(BF)
    value, slope = gelu_parts(branch_ref[...].astype(F32))
    states = state_f + state_b
    mixed_out_ref[...] = (value * states).astype(BF)
    branch_grad_ref[...] = (out_grad_ref[...] * states * slope).astype(BF)


def block_matrix(maps):
    heads = maps.shape[0]
    eye = jnp.eye(heads, dtype=maps.dtype)
    full = maps[:, :, None, :] * eye[:, None, :, None]
    return full.reshape(heads * maps.shape[1], heads * maps.shape[2])


def shards(
    cotangent,
    saved_input,
    routes,
    route_weight,
    gate_proj,
    up_proj,
    down_proj,
    out_proj,
    conv_input,
    gate_branch,
    conv_taps,
    recur_map,
    input_map,
    decay_param,
    decay_shift,
):
    length, width = cotangent.shape
    n = lax.axis_size("sp")
    n_tp = lax.axis_size("tp")
    experts = n * gate_proj.shape[0]
    slots = 4 * length // n
    slots = (slots + ROW_TILE - 1) // ROW_TILE * ROW_TILE
    fourth = width // n_tp
    channels = conv_input.shape[1]
    sds = jax.ShapeDtypeStruct

    sends, sendi, pick = local_call(
        functools.partial(prepare_kernel, slots),
        (cotangent, saved_input, routes.T, route_weight.T),
        (
            sds((experts, slots, fourth), BF),
            sds((experts, slots, fourth), BF),
            sds((experts * slots, length), BF),
        ),
    )
    got_scaled, got_input, halo = dispatch(sends, sendi, conv_input, n, n_tp)
    low, high = halo_edges(halo, n, 2)
    rows_scaled = got_scaled.reshape(experts * slots, width)
    rows_input = got_input.reshape(experts * slots, width)
    w_gate = gate_proj[0]
    w_up = up_proj[0]
    w_down = down_proj[0]
    gate_pre = jnp.dot(rows_input, w_gate, preferred_element_type=F32)
    up_pre = jnp.dot(rows_input, w_up, preferred_element_type=F32)
    gate_sig = jax.nn.sigmoid(gate_pre)
    gate_act = gate_pre * gate_sig
    hidden = (gate_act * up_pre).astype(BF)
    hidden_grad = lax.dot_general(
        rows_scaled, w_down, (((1,), (1,)), ((), ())), preferred_element_type=F32
    )
    gate_grad = (hidden_grad * up_pre * gate_sig * (1.0 + gate_pre * (1.0 - gate_sig))).astype(BF)
    up_grad = (hidden_grad * gate_act).astype(BF)
    partial_rows = lax.dot_general(
        gate_grad, w_gate, (((1,), (1,)), ((), ())), preferred_element_type=F32
    )
    partial_rows = partial_rows + lax.dot_general(
        up_grad, w_up, (((1,), (1,)), ((), ())), preferred_element_type=F32
    )
    part = partial_rows.astype(BF).reshape(experts, slots, width)
    normed_grad = send_back(part, pick, n, n_tp)
    rows0 = (((0,), (0,)), ((), ()))
    grad_down = lax.dot_general(hidden, rows_scaled, rows0, preferred_element_type=F32)
    grad_gate = lax.dot_general(rows_input, gate_grad, rows0, preferred_element_type=F32)
    grad_up = lax.dot_general(rows_input, up_grad, rows0, preferred_element_type=F32)

    maps = jnp.concatenate(
        [block_matrix(m[d]) for d in range(2) for m in (recur_map, input_map)], axis=1
    )
    plus = jax.nn.softplus(-decay_param)
    one = sds((length, channels), F32)
    two = sds((2, length, channels), F32)
    eight = sds((8, channels), F32)
    conv, gates, decay, root, state, cum, ones, tot, _ = local_call(
        pre_kernel,
        (conv_input, low, high, conv_taps, maps, plus, decay_shift),
        (one, sds((length, 4 * channels), F32), two, two, two, two, two, eight, two),
    )
    mixed_grad_b, out_grad, carried, after, tot2, _ = local_call(
        middle_kernel,
        (normed_grad, cotangent, saved_input, out_proj, gate_branch, decay, tot),
        (sds((length, width), BF), one, one, two, eight, two),
    )
    (everyone,) = exchange(tot2, n, True, 3)
    conv_grad, branch_grad, mixed_out, _ = local_call(
        functools.partial(last_kernel, n),
        (
            everyone, conv, gates, decay, root, state, cum, ones, after, carried, out_grad,
            gate_branch, maps, plus,
        ),
        (
            sds((length, channels), BF),
            sds((length, channels), BF),
            sds((length, channels), BF),
            sds((length, 4 * channels), F32),
        ),
    )
    grad_part = lax.dot_general(mixed_grad_b, mixed_out, rows0, preferred_element_type=F32)
    pieces, grad_halo = exchange(
        grad_part.astype(BF).reshape(n, width // n, channels), n, False, 4, conv_grad
    )
    grad_low, grad_high = halo_edges(grad_halo, n, 2)
    grad_out = jnp.sum(pieces.astype(F32), axis=0)
    taps32 = conv_taps.astype(F32)
    grad_pad = jnp.concatenate([grad_low, conv_grad, grad_high], axis=0).astype(F32)
    input_grad = jnp.zeros((length, channels), F32)
    for offset in range(taps32.shape[0]):
        input_grad = input_grad + grad_pad[4 - offset : 4 - offset + length] * taps32[offset]
    return (
        grad_gate[None],
        grad_up[None],
        grad_down[None],
        grad_out,
        input_grad.astype(BF),
        branch_grad,
    )


def solution(mesh):
    in_specs = (
        P("sp", None),
        P("sp", None),
        P("sp", None),
        P("sp", None),
        P("sp", None, "tp"),
        P("sp", None, "tp"),
        P("sp", "tp", None),
        P(None, "tp"),
        P("sp", "tp"),
        P("sp", "tp"),
        P(None, "tp"),
        P(None, "tp", None, None),
        P(None, "tp", None, None),
        P(None, "tp"),
        P(None, "sp", "tp"),
    )
    out_specs = (
        P("sp", None, "tp"),
        P("sp", None, "tp"),
        P("sp", "tp", None),
        P("sp", "tp"),
        P("sp", "tp"),
        P("sp", "tp"),
    )
    return jax.shard_map(shards, mesh=mesh, in_specs=in_specs, out_specs=out_specs, check_vma=False)
```

profile of v0, /device:TPU:0, one launch (start us, length us, event | category | flops | bytes accessed | tf_op | source)
XLA Modules:
  0.0 152.3 jit_solution(15918888977095110264)
XLA Ops:
  0.6 0.0 copy-start
  0.6 3.2 %shard_map.190 = (bf16[8,80,512]{2,1,0:T(8,128)(2,1)}, bf16[8,80,512]{2,1,0:T(8,128)(2,1)}, bf16[640,160]{1,0:T(8,128)(2,1)}) custom-call(bf16[160,2048]{1,0:T(8,128)(2,1)} %cot_ref.3, bf16[160,2048]{1,0:T(8,128)(2,1)} %x_ref.7, s32[2,160]{1,0:T(2,128)} %bitcast.71, f32[2,160]{1,0:T(2,128)} %bitcast.72), custom_call_target="tpu_custom_call" | custom-call | flops 10000000 | bytes 4000000 | tf_op jit(solution)/shard_map/pallas_call | solution.py:20
  3.9 0.0 copy-start.2
  3.9 1.1 copy-done.2
  5.0 0.0 copy-start.3
  5.0 1.1 copy-done.3
  6.1 0.0 copy-start.6
  6.1 0.9 copy-done.6
  6.9 48.6 %shard_map.191 = (bf16[8,80,2048]{2,1,0:T(8,128)(2,1)S(1)}, bf16[8,80,2048]{2,1,0:T(8,128)(2,1)S(1)}, bf16[2,16,256]{2,1,0:T(8,128)(2,1)S(1)}) custom-call(bf16[8,80,512]{2,1,0:T(8,128)(2,1)S(1)} %copy-done.2, bf16[8,80,512]{2,1,0:T(8,128)(2,1)S(1)} %copy-done.3, bf16[160,256]{1,0:T(8,128)(2,1)S(1)} %copy-done.6), custom_call_target="tpu_custom_call" | custom-call | bytes 100000000 | tf_op jit(solution)/shard_map/pallas_call | solution.py:213
  55.5 0.0 copy-done
  55.5 0.0 copy-start.10
  55.5 0.8 fusion.2
  56.4 0.4 copy-done.10
  56.7 0.0 copy-start.16
  56.7 0.8 fusion.5
  57.6 0.4 copy-done.16
  58.0 1.0 multiply_convert_fusion.1
  59.0 2.3 %convolution_bitcast_fusion.2 = f32[1,2048,256]{2,1,0:T(8,128)} fusion(bf16[640,2048]{1,0:T(8,128)(2,1)S(1)} %bitcast.65, bf16[640,256]{1,0:T(8,128)(2,1)S(1)} %get-tuple-element.55), kind=kOutput, calls=%fused_computation.3 | convolution fusion | flops 671088640 | bytes 5046272 | tf_op jit(solution)/shard_map/dot_general | solution.py:623
  61.3 2.3 %convolution_bitcast_fusion.1 = f32[1,2048,256]{2,1,0:T(8,128)} fusion(bf16[640,2048]{1,0:T(8,128)(2,1)S(1)} %bitcast.66, bf16[640,256]{1,0:T(8,128)(2,1)S(1)} %get-tuple-element.54), kind=kOutput, calls=%fused_computation.2 | convolution fusion | flops 671088640 | bytes 5046272 | tf_op jit(solution)/shard_map/dot_general | solution.py:624
  63.7 2.4 %convolution_bitcast_fusion = f32[1,256,2048]{2,1,0:T(8,128)} fusion(bf16[640,2048]{1,0:T(8,128)(2,1)S(1)} %bitcast.62, f32[640,256]{1,0:T(8,128)S(1)} %fusion.5, f32[640,256]{1,0:T(8,128)S(1)} %fusion.2), kind=kOutput, calls=%fused_computation.1 | convolution fusion | flops 672071680 | bytes 6029312 | tf_op jit(solution)/shard_map/dot_general | solution.py:622
  66.0 0.9 fusion
  66.9 0.0 copy-start.5
  66.9 0.9 add_convert_fusion
  67.8 0.0 copy-start.12
  67.8 0.0 copy-start.13
  67.8 0.1 copy-done.5
  67.9 29.9 %shard_map.192.ng_ref = bf16[160,2048]{1,0:T(8,128)(2,1)S(1)} custom-call(bf16[8,80,2048]{2,1,0:T(8,128)(2,1)S(1)} %bitcast.59, bf16[640,160]{1,0:T(8,128)(2,1)S(1)} %copy-done.5), custom_call_target="tpu_custom_call" | custom-call | bytes 100000000 | tf_op jit(solution)/shard_map/pallas_call | solution.py:311
  97.8 0.0 copy-start.1
  97.8 0.8 copy-done.1
  98.6 0.0 copy-start.15
  98.6 0.6 fusion.18
  99.2 0.0 copy-done.12
  99.2 0.0 copy-done.13
  99.3 0.6 broadcast_multiply_fusion
  99.8 0.2 mul.148
  100.1 0.2 mul.152
  100.3 0.2 mul.156
  100.5 0.2 mul.160
  100.8 0.0 copy-done.15
  100.8 0.0 copy-start.9
  100.8 0.6 compare_select_fusion.plus_ref
  101.4 0.2 copy-done.9
  101.6 4.6 %shard_map.193 = (f32[160,256]{1,0:T(8,128)}, f32[160,1024]{1,0:T(8,128)}, f32[2,160,256]{2,1,0:T(8,128)}, f32[2,160,256]{2,1,0:T(8,128)}, f32[2,160,256]{2,1,0:...) custom-call(bf16[160,256]{1,0:T(8,128)(2,1)} %x_ref.6, ...), custom_call_target="tpu_custom_call" | custom-call | flops 10000000 | bytes 4000000 | tf_op jit(solution)/shard_map/pallas_call | solution.py:20
  106.2 4.5 %shard_map.194 = (bf16[160,2048]{1,0:T(8,128)(2,1)}, f32[160,256]{1,0:T(8,128)}, f32[160,256]{1,0:T(8,128)}, f32[2,160,256]{2,1,0:T(8,128)}, f32[8,256]{1,0:T(8,128)}, /*index=5*/f32[2,160,256]{2,1,0:T(8,128)}) custom-call(bf16[160,2048]{1,0:T(8,128)(2,1)} %copy-done.1, bf16[160,2048]{1,0:T(8,128)(2,1)} %cot_ref.3, bf16[160,2048]{1,0:T(8,128)(2,1)} %x_ref.7, ...), custom_call_target="tpu_custom_call" | custom-call | flops 10000000 | bytes 4000000 | tf_op jit(solution)/shard_map/pallas_call | solution.py:20
  110.7 0.0 copy-start.8
  110.7 0.7 copy-done.8
  111.4 0.0 copy-start.11
  111.4 6.5 %shard_map.195.all_ref = f32[8,8,256]{2,1,0:T(8,128)S(1)} custom-call(f32[8,256]{1,0:T(8,128)S(1)} %copy-done.8), custom_call_target="tpu_custom_call" | custom-call | bytes 20000000 | tf_op jit(solution)/shard_map/pallas_call | solution.py:360
  118.0 0.0 copy-start.7
  118.0 0.6 copy-done.7
  118.6 3.7 %shard_map.196 = (bf16[160,256]{1,0:T(8,128)(2,1)}, bf16[160,256]{1,0:T(8,128)(2,1)}, bf16[160,256]{1,0:T(8,128)(2,1)}, f32[160,1024]{1,0:T(8,128)}) custom-call(f32[8,8,256]{2,1,0:T(8,128)} %copy-done.7, f32[160,256]{1,0:T(8,128)} %get-tuple-element.40.conv_ref, f32[160,1024]{1,0:T(8,128)} %get-tuple-element.41.gates_ref, ...), custom_call_target="tpu_custom_call" | custom-call | flops 10000000 | bytes 4000000 | tf_op jit(solution)/shard_map/pallas_call | solution.py:20
  122.3 0.0 copy-start.14
  122.3 0.0 copy-done.11
  122.3 1.4 convolution_convert_fusion
  123.7 0.0 copy-start.4
  123.7 0.9 copy-done.4
  124.6 26.1 %shard_map.197 = (bf16[8,256,256]{2,1,0:T(8,128)(2,1)S(1)}, bf16[2,16,256]{2,1,0:T(8,128)(2,1)S(1)}) custom-call(bf16[8,256,256]{2,1,0:T(8,128)(2,1)S(1)} %bitcast.60, bf16[160,256]{1,0:T(8,128)(2,1)S(1)} %copy-done.4), custom_call_target="tpu_custom_call" | custom-call | bytes 20000000 | tf_op jit(solution)/shard_map/pallas_call | solution.py:360
  150.7 0.8 convert_reduce_fusion
  151.6 0.0 copy-done.14
  151.6 0.7 fusion.11
  (9 shorter events, 0.1 us)
Async XLA Ops:
  0.6 54.9 %copy-start = (bf16[1,2048,256]{2,1,0:T(8,128)(2,1)S(1)}, bf16[1,2048,256]{2,1,0:T(8,128)(2,1)}, u32[]{:S(2)}) copy-start(bf16[1,2048,256]{2,1,0:T(8,128)(2,1)} %param.19) | copy-start | bytes 3145732
  3.9 1.1 copy-start.2
  5.0 1.1 copy-start.3
  6.1 0.9 copy-start.6
  55.5 1.2 copy-start.10
  56.7 1.2 copy-start.16
  66.9 1.0 copy-start.5
  67.8 31.4 %copy-start.12 = (bf16[2,4,64,64]{3,2,1,0:T(8,128)(2,1)S(1)}, bf16[2,4,64,64]{3,2,1,0:T(8,128)(2,1)}, u32[]{:S(2)}) copy-start(bf16[2,4,64,64]{3,2,1,0:T(8,128)(2,1)} %param.27) | copy-start | bytes 196612
  67.8 31.4 %copy-start.13 = (bf16[2,4,64,64]{3,2,1,0:T(8,128)(2,1)S(1)}, bf16[2,4,64,64]{3,2,1,0:T(8,128)(2,1)}, u32[]{:S(2)}) copy-start(bf16[2,4,64,64]{3,2,1,0:T(8,128)(2,1)} %param.26) | copy-start | bytes 196612
  97.8 0.9 copy-start.1
  98.6 2.1 %copy-start.15 = (f32[2,256]{1,0:T(2,128)S(1)}, f32[2,256]{1,0:T(2,128)}, u32[]{:S(2)}) copy-start(f32[2,256]{1,0:T(2,128)} %param.28) | copy-start | bytes 6148
  100.8 0.8 copy-start.9
  110.7 0.7 copy-start.8
  111.4 10.9 %copy-start.11 = (bf16[160,2048]{1,0:T(8,128)(2,1)S(1)}, bf16[160,2048]{1,0:T(8,128)(2,1)}, u32[]{:S(2)}) copy-start(bf16[160,2048]{1,0:T(8,128)(2,1)} %get-tuple-element.38) | copy-start | bytes 1966084
  118.0 0.6 copy-start.7
  122.3 29.3 %copy-start.14 = (bf16[4,256]{1,0:T(4,128)(2,1)S(1)}, bf16[4,256]{1,0:T(4,128)(2,1)}, u32[]{:S(2)}) copy-start(bf16[4,256]{1,0:T(4,128)(2,1)} %taps_ref.1) | copy-start | bytes 6148
  123.7 0.9 copy-start.4
where the time goes:
time: 153 us; the launch traced here: 152 us
  Pallas kernels  127 us (83%)
  matrix products  12.8 us (8%)
  local copies, waits for them, and re-layouts  8.01 us (5%)
  other arithmetic  3.41 us (2%)
    pallas_call x1, Pallas kernels, dispatch(): pl.pallas_call(functools.partial(dispatch_kernel, n), out_shape=(full, fu...  48.6 us
    pallas_call x2, Pallas kernels, exchange(): pl.pallas_call(functools.partial(exchange_kernel, n, same, edges is not N...  32.6 us
    pallas_call x1, Pallas kernels, send_back(): pl.pallas_call(functools.partial(return_kernel, n), out_shape=jax.ShapeDt...  29.9 us
    pallas_call x4, Pallas kernels, local_call(): pl.pallas_call(kernel, out_shape=outs, in_specs=[VM] * len(args), out_spe...  16.1 us
    unnamed x37, local copies, waits for them, and re-layouts  7.12 us

commit v1 on v0

v1 whole, which is shorter than its diff:
```python
import functools
import jax
import jax.numpy as jnp
from jax import lax
from jax.experimental import pallas as pl
from jax.experimental.pallas import tpu as pltpu
from jax.sharding import PartitionSpec as P

EPS = 1e-06
DECAY_SCALE = 8.0
ROW_TILE = 16
GROUPS = 4
LAG = 2
GELU_K = 0.7978845608028654
GELU_C = 0.044715
VM = pl.BlockSpec(memory_space=pltpu.VMEM)
HB = pl.BlockSpec(memory_space=pltpu.HBM)
BF = jnp.bfloat16
F32 = jnp.float32
ROWS0 = (((0,), (0,)), ((), ()))
COLS1 = (((1,), (1,)), ((), ()))
PLAIN = (((1,), (0,)), ((), ()))


def neighbours():
    tp = lax.axis_index("tp")
    side = tp // 2
    core = tp % 2
    return tp, side * 2 + (1 - core), (1 - side) * 2 + core, (1 - side) * 2 + (1 - core)


def partner_at(sp, n, d):
    if n & (n - 1):
        return (sp + d) % n
    bit, peer = 1, sp
    while bit < n:
        if d & bit:
            peer = peer + bit * (1 - 2 * ((sp // bit) % 2))
        bit *= 2
    return peer


def source_at(sp, n, d):
    return (sp + n - d) % n if n & (n - 1) else partner_at(sp, n, d)


def announce(n, tps):
    sp = lax.axis_index("sp")
    tp = lax.axis_index("tp")
    barrier = pltpu.get_barrier_semaphore()
    for d in range(1, n):
        pl.semaphore_signal(
            barrier, inc=1, device_id=((sp + d) % n, tp), device_id_type=pl.DeviceIdType.MESH
        )
    for other in tps:
        pl.semaphore_signal(barrier, inc=1, device_id=(sp, other), device_id_type=pl.DeviceIdType.MESH)
    return barrier, n - 1 + len(tps)


def remote(src, dst, sems, index, device):
    return pltpu.make_async_remote_copy(
        src_ref=src,
        dst_ref=dst,
        send_sem=sems.at[(0,) + index],
        recv_sem=sems.at[(1,) + index],
        device_id=device,
        device_id_type=pl.DeviceIdType.MESH,
    )


def edge_copies(n, x_ref, halo_ref, sems):
    sp = lax.axis_index("sp")
    tp = lax.axis_index("tp")
    length, tile = x_ref.shape[0], halo_ref.shape[1]
    copies = (
        remote(x_ref.at[pl.ds(length - tile, tile)], halo_ref.at[0], sems, (0,), ((sp + 1) % n, tp)),
        remote(x_ref.at[pl.ds(0, tile)], halo_ref.at[1], sems, (1,), ((sp + n - 1) % n, tp)),
    )
    for copy in copies:
        copy.start()
    return copies


def halo_rows(halo_ref, n):
    sp = lax.axis_index("sp")
    before = jnp.where(sp == 0, 0.0, halo_ref[0].astype(F32))
    after = jnp.where(sp == n - 1, 0.0, halo_ref[1].astype(F32))
    return before[before.shape[0] - 2 :], after[:2]


def split_dot(x, w, dims):
    high = x.astype(BF)
    low = (x - high.astype(F32)).astype(BF)
    total = lax.dot_general(low, w, dims, preferred_element_type=F32)
    return total + lax.dot_general(high, w, dims, preferred_element_type=F32)


def minus_expm1(y):
    series = 1.0 + y * (1.0 / 8.0)
    for k in (7.0, 6.0, 5.0, 4.0, 3.0, 2.0):
        series = 1.0 + y * (1.0 / k) * series
    return jnp.where(y > -0.25, -y * series, 1.0 - jnp.exp(y))


def shifted(x, by, edge):
    length = x.shape[0]
    row = lax.broadcasted_iota(jnp.int32, x.shape, 0)
    moved = pltpu.roll(x, by % length, 0)
    return jnp.where(row == (0 if by > 0 else length - 1), edge, moved)


def run_scans(length, jobs):
    width = jobs[0][1].shape[1]
    groups = length // 8

    def body(g, carry):
        out = []
        for (reverse, a_ref, b_ref, to_ref), state in zip(jobs, carry):
            base = pl.multiple_of((groups - 1 - g if reverse else g) * 8, 8)
            a = a_ref[pl.ds(base, 8), :]
            b = None if b_ref is None else b_ref[pl.ds(base, 8), :]
            rows = [None] * 8
            for k in reversed(range(8)) if reverse else range(8):
                state = a[k : k + 1] * state
                if b is not None:
                    state = state + b[k : k + 1]
                rows[k] = state
            to_ref[pl.ds(base, 8), :] = jnp.concatenate(rows, axis=0)
            out.append(state)
        return tuple(out)

    start = tuple(
        jnp.full((1, width), 1.0 if b_ref is None else 0.0, F32) for _, _, b_ref, _ in jobs
    )
    return lax.fori_loop(0, groups, body, start)


def gelu_parts(x):
    t = jnp.tanh(GELU_K * (x + GELU_C * x * x * x))
    value = 0.5 * x * (1.0 + t)
    slope = 0.5 * (1.0 + t) + 0.5 * x * (1.0 - t * t) * GELU_K * (1.0 + 3.0 * GELU_C * x * x)
    return value, slope


def carries(n, all_ref, rows):
    sp = lax.axis_index("sp")
    zero = jnp.zeros((1, all_ref.shape[2]), F32)
    (lp, le), (up, ue) = rows

    def lower(k, carry):
        t = all_ref[k]
        return t[lp : lp + 1] * carry + t[le : le + 1]

    def upper(i, carry):
        t = all_ref[n - 1 - i]
        return t[up : up + 1] * carry + t[ue : ue + 1]

    return lax.fori_loop(0, sp, lower, zero), lax.fori_loop(0, n - 1 - sp, upper, zero)


def front_kernel(n, slots, *refs):
    (
        cot_hbm, x_hbm, routes_ref, weight_ref, wg_hbm, wu_hbm, wd_hbm, cin_ref, branch_ref,
        taps_ref, rmap_ref, imap_ref, plus_ref, shift_hbm,
        ng_ref, ggate_ref, gup_ref, gdown_ref,
        maps_ref, decay_ref, ones_ref, a_ref, c_ref, e_ref, value_ref, slope_ref, mixed_out_ref,
        tot_ref,
        cot_ref, x_ref, nx_ref, wg_ref, wu_ref, wd_ref, shift_ref,
        rank_ref, pick_ref, send_ref, wide_ref, rows_sc, rows_in, hid_ref, ggu_ref, part_ref,
        got1, got2, mid, fin, back, halo_ref,
        conv_ref, gates_ref, root_ref, drive_ref, state_ref, cum_ref, all_ref,
        loc, edge, hop, wide, pair, cross, fwd, s_pair, s_cross, s_hop, s_tail, s_tot,
    ) = refs
    length, width = cot_ref.shape
    fourth = send_ref.shape[3]
    channels = cin_ref.shape[1]
    sp = lax.axis_index("sp")
    tp, partner, across, diagonal = neighbours()
    per = n // GROUPS
    rows = (rows_sc, rows_in)

    def cols(q):
        return pl.ds(pl.multiple_of(q * fourth, 128), fourth)

    barrier, heard = announce(n, (partner, across))
    loads = [
        pltpu.make_async_copy(src, dst, loc.at[i])
        for i, (src, dst) in enumerate(
            (
                (x_hbm, x_ref), (cot_hbm, cot_ref), (shift_hbm, shift_ref),
                (wg_hbm, wg_ref), (wu_hbm, wu_ref), (wd_hbm, wd_ref),
            )
        )
    ]
    for load in loads:
        load.start()

    route0, route1 = routes_ref[0:1], routes_ref[1:2]
    which = lax.broadcasted_iota(jnp.int32, (n, length), 0)
    named = ((which == route0) | (which == route1)).astype(F32).astype(BF)
    earlier = lax.broadcasted_iota(jnp.int32, (length, length), 0) < lax.broadcasted_iota(
        jnp.int32, (length, length), 1
    )
    rank_ref[...] = jnp.dot(named, earlier.astype(F32).astype(BF), preferred_element_type=F32)
    loads[0].wait()
    for r in range(0, length, 32):
        x = x_ref[r : r + 32].astype(F32)
        inv = lax.rsqrt(jnp.mean(x * x, axis=1, keepdims=True) + EPS)
        nx_ref[r : r + 32] = (x * inv).astype(BF)
    loads[1].wait()

    def chosen(d):
        e = partner_at(sp, n, d)
        rank = rank_ref[pl.ds(e, 1), :].astype(jnp.int32)
        slot = lax.broadcasted_iota(jnp.int32, (slots, length), 0) == rank
        hit0 = slot & (route0 == e)
        hit1 = slot & (route1 == e)
        pick = (hit0 | hit1).astype(F32).astype(BF)
        pick_ref[d * slots : (d + 1) * slots] = pick
        share = jnp.where(hit0, weight_ref[0:1], 0.0) + jnp.where(hit1, weight_ref[1:2], 0.0)
        return pick, jnp.sum(share, axis=1, keepdims=True)

    def taken(pick, share, where):
        got = jnp.dot(pick, nx_ref[:, where], preferred_element_type=F32).astype(BF)
        cot = jnp.dot(pick, cot_ref[:, where], preferred_element_type=F32)
        return (cot * share).astype(BF), got

    near_d = [d for d in (1,) if d < n]
    far = [d for d in range(2, n)]
    order = near_d + [d for g in range(GROUPS - 1, -1, -1) for d in far if d // per == g]
    hops, extra, pending = {}, {}, []
    pl.semaphore_wait(barrier, heard)
    edges = edge_copies(n, cin_ref, halo_ref, edge)
    for d in order:
        peer = partner_at(sp, n, d)
        pick, share = chosen(d)
        for a, value in enumerate(taken(pick, share, cols(tp))):
            send_ref[a, d] = value
            copy = remote(send_ref.at[a, d], rows[a].at[d, :, cols(tp)], hop, (a, d), (peer, tp))
            copy.start()
            hops[a, d] = copy
        if d in near_d:
            for a, value in enumerate(taken(pick, share, cols(across))):
                i = near_d.index(d)
                wide_ref[a, i] = value
                copy = remote(
                    wide_ref.at[a, i], rows[a].at[d, :, cols(across)], wide, (a, i), (peer, tp)
                )
                copy.start()
                extra[a, d] = copy
    pick, share = chosen(0)
    for q in range(width // fourth):
        where = pl.ds(q * fourth, fourth)
        rows_sc[0, :, where], rows_in[0, :, where] = taken(pick, share, where)

    heads, hw = rmap_ref.shape[1], rmap_ref.shape[2]
    spread = (
        lax.broadcasted_iota(jnp.int32, (hw, channels), 1) % hw
        == lax.broadcasted_iota(jnp.int32, (hw, channels), 0)
    ).astype(F32).astype(BF)
    block = (
        lax.broadcasted_iota(jnp.int32, (channels, channels), 0) // hw
        == lax.broadcasted_iota(jnp.int32, (channels, channels), 1) // hw
    )
    for i in range(4):
        stack = (rmap_ref, imap_ref)[i % 2][i // 2].reshape(heads * hw, hw)
        full = jnp.dot(stack, spread, preferred_element_type=F32)
        maps_ref[:, i * channels : (i + 1) * channels] = jnp.where(block, full, 0.0).astype(BF)
    for copy in edges:
        copy.wait()
    taps = taps_ref[...].astype(F32)
    low, high = halo_rows(halo_ref, n)
    x = cin_ref[...].astype(F32)
    back1 = shifted(x, 1, low[1:2])
    back2 = shifted(back1, 1, low[0:1])
    conv = back2 * taps[0:1] + back1 * taps[1:2] + x * taps[2:3]
    conv = conv + shifted(x, -1, high[0:1]) * taps[3:4]
    conv_ref[...] = conv
    gates_ref[...] = jax.nn.sigmoid(split_dot(conv, maps_ref[...], PLAIN))
    loads[2].wait()
    for d in range(2):
        recur = gates_ref[:, 2 * d * channels : (2 * d + 1) * channels]
        inputs = gates_ref[:, (2 * d + 1) * channels : (2 * d + 2) * channels]
        log_decay = -DECAY_SCALE * recur * plus_ref[d : d + 1, :] + shift_ref[d]
        root = jnp.sqrt(minus_expm1(2.0 * log_decay))
        decay_ref[d] = jnp.exp(log_decay)
        root_ref[d] = root
        drive_ref[d] = root * (inputs * conv_ref[...])
    a_f, a_b = decay_ref.at[0], decay_ref.at[1]
    ends = run_scans(
        length,
        (
            (False, a_f, drive_ref.at[0], state_ref.at[0]),
            (True, a_b, drive_ref.at[1], state_ref.at[1]),
            (False, a_f, None, cum_ref.at[0]),
            (True, a_b, None, cum_ref.at[1]),
            (True, a_f, None, ones_ref.at[0]),
            (False, a_b, None, ones_ref.at[1]),
        ),
    )
    tot_ref[0:1, :] = ends[2]
    tot_ref[1:2, :] = ends[0]
    tot_ref[2:3, :] = ends[3]
    tot_ref[3:4, :] = ends[1]
    tot_ref[4:8, :] = jnp.zeros((4, channels), F32)
    totals = []
    for d in range(n - 1, 0, -1):
        copy = remote(tot_ref, all_ref.at[sp], s_tot, (d,), (partner_at(sp, n, d), tp))
        copy.start()
        totals.append(copy)
    all_ref[sp] = tot_ref[...]

    def finish_states():
        for copy in totals:
            copy.wait()
        in_f, in_b = carries(n, all_ref, ((0, 1), (2, 3)))
        state_f = state_ref[0] + cum_ref[0] * in_f
        state_b = state_ref[1] + cum_ref[1] * in_b
        beside = (shifted(state_f, 1, in_f), shifted(state_b, -1, in_b))
        value, slope = gelu_parts(branch_ref[...].astype(F32))
        states = state_f + state_b
        value_ref[...] = value
        slope_ref[...] = states * slope
        mixed_out_ref[...] = (value * states).astype(BF)
        conv = conv_ref[...]
        for d in range(2):
            recur = gates_ref[:, 2 * d * channels : (2 * d + 1) * channels]
            inputs = gates_ref[:, (2 * d + 1) * channels : (2 * d + 2) * channels]
            decay = decay_ref[d]
            root = root_ref[d]
            a_ref[d] = root * inputs
            g_log = beside[d] * decay - inputs * conv * (decay * decay) / root
            c_ref[d] = g_log * (-DECAY_SCALE * plus_ref[d : d + 1, :]) * recur * (1.0 - recur)
            e_ref[d] = root * conv * inputs * (1.0 - inputs)

    nears, fwds, overs, late = {}, {}, {}, []

    def step_in(a, d):
        hops[a, d].wait_recv()
        dst = rows[a]
        mine = dst.at[d, :, cols(tp)]
        if d in near_d:
            extra[a, d].wait_recv()
            other = dst.at[d, :, cols(across)]
            fwds[a, d] = remote(other, other, fwd, (a, d), (sp, partner))
            fwds[a, d].start()
        else:
            overs[a, d] = remote(mine, mine, cross, (a, d), (sp, across))
            overs[a, d].start()
            late.append((a, d))
        nears[a, d] = remote(mine, mine, pair, (a, d), (sp, partner))
        nears[a, d].start()

    def step_on():
        a, d = late.pop(0)
        overs[a, d].wait_recv()
        other = rows[a].at[d, :, cols(across)]
        fwds[a, d] = remote(other, other, fwd, (a, d), (sp, partner))
        fwds[a, d].start()

    def bring(g):
        for d in order:
            if d // per == g:
                for a in range(2):
                    step_in(a, d)
                    if len(late) > LAG:
                        step_on()

    pairs, crosses, backs = {}, {}, {}

    def experts(g):
        while any(d // per == g for _, d in late):
            step_on()
        for d in range(g * per, (g + 1) * per):
            if d:
                for a in range(2):
                    nears[a, d].wait_recv()
                    fwds[a, d].wait_recv()
        count = per * slots
        at = slice(g * count, (g + 1) * count)
        xin = rows_in[g * per : (g + 1) * per].reshape(count, width)
        gate_pre = jnp.dot(xin, wg_ref[...], preferred_element_type=F32)
        up_pre = jnp.dot(xin, wu_ref[...], preferred_element_type=F32)
        xsc = rows_sc[g * per : (g + 1) * per].reshape(count, width)
        hidden_grad = lax.dot_general(xsc, wd_ref[...], COLS1, preferred_element_type=F32)
        gate_sig = jax.nn.sigmoid(gate_pre)
        gate_act = gate_pre * gate_sig
        hid_ref[at] = (gate_act * up_pre).astype(BF)
        gate_grad = hidden_grad * up_pre * gate_sig * (1.0 + gate_pre * (1.0 - gate_sig))
        gate_grad = gate_grad.astype(BF)
        up_grad = (hidden_grad * gate_act).astype(BF)
        units = up_grad.shape[1]
        ggu_ref[at, :units] = gate_grad
        ggu_ref[at, units:] = up_grad
        for i, q in enumerate((diagonal, partner, across, tp)):
            some = pl.ds(pl.multiple_of(q * fourth, 128), fourth)
            total = lax.dot_general(gate_grad, wg_ref[some], COLS1, preferred_element_type=F32)
            total = total + lax.dot_general(up_grad, wu_ref[some], COLS1, preferred_element_type=F32)
            part_ref[g * per : (g + 1) * per, :, cols(q)] = total.astype(BF).reshape(
                per, slots, fourth
            )
            if i < 2:
                for d in range(g * per, (g + 1) * per):
                    copy = remote(
                        part_ref.at[d, :, cols(q)], got1.at[i, d], s_pair, (i, d), (sp, partner)
                    )
                    copy.start()
                    pairs[i, d] = copy

    def stage_b(g):
        for d in range(g * per, (g + 1) * per):
            pairs[0, d].wait_recv()
            total = part_ref[d, :, cols(across)].astype(F32) + got1[0, d].astype(F32)
            mid[d] = total.astype(BF)
            crosses[d] = remote(mid.at[d], got2.at[d], s_cross, (d,), (sp, across))
            crosses[d].start()

    def stage_c(g):
        for d in range(g * per, (g + 1) * per):
            pairs[1, d].wait_recv()
            crosses[d].wait_recv()
            total = part_ref[d, :, cols(tp)].astype(F32) + got1[1, d].astype(F32)
            total = (total + got2[d].astype(F32)).astype(BF)
            if d == 0:
                back[0] = total
            else:
                fin[d] = total
                backs[d] = remote(fin.at[d], back.at[d], s_hop, (d,), (source_at(sp, n, d), tp))
                backs[d].start()

    chunk = width // 8

    def weight_gradients(k):
        at = slice(k * chunk, (k + 1) * chunk)
        units = hid_ref.shape[1]
        left = rows_in[:, :, at].reshape(n * slots, chunk)
        both = lax.dot_general(left, ggu_ref[...], ROWS0, preferred_element_type=F32)
        ggate_ref[at] = both[:, :units]
        gup_ref[at] = both[:, units:]
        right = rows_sc[:, :, at].reshape(n * slots, chunk)
        gdown_ref[:, at] = lax.dot_general(hid_ref[...], right, ROWS0, preferred_element_type=F32)

    bring(0)
    bring(3)
    for i in (3, 4, 5):
        loads[i].wait()
    experts(0)
    bring(2)
    experts(3)
    stage_b(0)
    bring(1)
    experts(2)
    stage_b(3)
    stage_c(0)
    experts(1)
    stage_b(2)
    stage_c(3)
    stage_b(1)
    weight_gradients(0)
    weight_gradients(1)
    stage_c(2)
    weight_gradients(2)
    weight_gradients(3)
    stage_c(1)
    finish_states()
    for k in range(4, 8):
        weight_gradients(k)
    for d in range(1, n):
        backs[d].wait_recv()
    got = back[...].reshape(n * slots, fourth)
    grad = lax.dot_general(pick_ref[...], got, ROWS0, preferred_element_type=F32)
    ng_ref[:, cols(tp)] = grad.astype(BF)
    own = ng_ref.at[:, cols(tp)]
    over = remote(own, own, s_tail, (0,), (sp, across))
    near = remote(own, own, s_tail, (1,), (sp, partner))
    over.start()
    near.start()
    over.wait_recv()
    other = ng_ref.at[:, cols(across)]
    last = remote(other, other, s_tail, (2,), (sp, partner))
    last.start()
    for group in (hops, extra, nears, fwds, overs, pairs, crosses, backs):
        for copy in group.values():
            copy.wait_send()
    near.wait()
    over.wait_send()
    last.wait()


def front(args, plus, shapes, n, n_tp, slots):
    cot, x, routes, weight, wg, wu, wd, cin, branch, taps, rmap, imap, shift = args
    length, width = cot.shape
    channels = cin.shape[1]
    units = wg.shape[1]
    fourth = width // n_tp
    dma = pltpu.SemaphoreType.DMA
    sds = jax.ShapeDtypeStruct
    vm = pltpu.VMEM
    one, two = (length, channels), (2, length, channels)
    outs = (
        sds((length, width), BF),
        sds((width, units), F32),
        sds((width, units), F32),
        sds((units, width), F32),
        sds((channels, 4 * channels), BF),
        sds(two, F32), sds(two, F32), sds(two, F32), sds(two, F32), sds(two, F32),
        sds(one, F32), sds(one, F32), sds(one, BF),
        sds((8, channels), F32),
    )
    block = (n, slots, fourth)
    scratch = [
        vm((length, width), BF), vm((length, width), BF), vm((length, width), BF),
        vm((width, units), BF), vm((width, units), BF), vm((units, width), BF), vm(two, F32),
        vm((n, length), F32), vm((n * slots, length), BF), vm((2,) + block, BF),
        vm((2, 1, slots, fourth), BF),
        vm((n, slots, width), BF), vm((n, slots, width), BF),
        vm((n * slots, units), BF), vm((n * slots, 2 * units), BF), vm((n, slots, width), BF),
        vm((2,) + block, BF), vm(block, BF), vm(block, BF), vm(block, BF), vm(block, BF),
        vm((2, ROW_TILE, channels), BF),
        vm(one, F32), vm((length, 4 * channels), F32), vm(two, F32), vm(two, F32), vm(two, F32),
        vm(two, F32), vm((n, 8, channels), F32),
        dma((6,)), dma((2, 2)), dma((2, 2, n)), dma((2, 2, 1)), dma((2, 2, n)), dma((2, 2, n)),
        dma((2, 2, n)), dma((2, 2, n)), dma((2, n)), dma((2, n)), dma((2, 3)), dma((2, n)),
    ]
    return pl.pallas_call(
        functools.partial(front_kernel, n, slots),
        out_shape=outs,
        in_specs=[HB, HB, VM, VM, HB, HB, HB, VM, VM, VM, VM, VM, VM, HB],
        out_specs=[VM] * len(outs),
        scratch_shapes=scratch,
        compiler_params=pltpu.CompilerParams(
            collective_id=1, has_side_effects=True, vmem_limit_bytes=40 * 2**20
        ),
        cost_estimate=pl.CostEstimate(
            flops=2_000_000_000, bytes_accessed=30_000_000, transcendentals=0
        ),
    )(cot, x, routes, weight, wg, wu, wd, cin, branch, taps, rmap, imap, plus, shift)


def tail_kernel(n, *refs):
    (
        ng_ref, cot_ref, x_ref, proj_ref, decay_ref, ones_ref, a_ref, c_ref, e_ref, value_ref,
        slope_ref, maps_ref, tot_ref, mixed_out_ref, taps_ref,
        grad_out_ref, input_grad_ref, branch_grad_ref,
        mixed_ref, mixed_all, out_all, drive_ref, after_ref, msg_ref, all_ref, packed_ref,
        conv_grad_ref, halo_ref,
        s_tot, s_mix, s_pair, s_out, s_edge,
    ) = refs
    length, width = ng_ref.shape
    channels = decay_ref.shape[2]
    part = width // n
    half = length // 2
    sp = lax.axis_index("sp")
    tp, partner, _, _ = neighbours()
    barrier, heard = announce(n, (partner,))
    powers = n & (n - 1) == 0
    mine = pl.ds(pl.multiple_of((tp % 2) * half, ROW_TILE), half)

    out_all[0] = mixed_out_ref[...]
    pl.semaphore_wait(barrier, heard)
    gathers = []

    def gather(bit):
        got = []
        for d in range(0, n, 2 * bit):
            copy = remote(out_all.at[d], out_all.at[d + bit], s_out, (d + bit,), (partner_at(sp, n, bit), tp))
            copy.start()
            got.append(copy)
        gathers.append(got)

    bits = []
    if powers:
        bit = n // 2
        while bit:
            bits.append(bit)
            bit //= 2
        gather(bits.pop(0))
    else:
        got = []
        for d in range(1, n):
            copy = remote(out_all.at[0], out_all.at[d], s_out, (d,), (partner_at(sp, n, d), tp))
            copy.start()
            got.append(copy)
        gathers.append(got)

    def gather_on():
        if bits:
            for copy in gathers[-1]:
                copy.wait_recv()
            gather(bits.pop(0))

    for r in range(0, length, 32):
        x = x_ref[r : r + 32].astype(F32)
        inv = lax.rsqrt(jnp.mean(x * x, axis=1, keepdims=True) + EPS)
        normed = x * inv
        ng = ng_ref[r : r + 32].astype(F32)
        dot = jnp.mean(ng * normed, axis=1, keepdims=True)
        mixed = (cot_ref[r : r + 32].astype(F32) + inv * (ng - normed * dot)).astype(BF)
        for e in range(n):
            mixed_ref[e, r : r + 32] = mixed[:, e * part : (e + 1) * part]
    out_grad = jnp.zeros((length, channels), F32)
    for e in range(n):
        out_grad = out_grad + jnp.dot(
            mixed_ref[e], proj_ref[e * part : (e + 1) * part], preferred_element_type=F32
        )
    carried = out_grad * value_ref[...]
    branch_grad_ref[...] = (out_grad * slope_ref[...]).astype(BF)
    drive_ref[...] = decay_ref[...] * carried[None]
    ends = run_scans(
        length,
        (
            (True, decay_ref.at[0], drive_ref.at[0], after_ref.at[0]),
            (False, decay_ref.at[1], drive_ref.at[1], after_ref.at[1]),
        ),
    )
    msg_ref[0:1, :] = tot_ref[0:1, :]
    msg_ref[1:2, :] = tot_ref[2:3, :]
    msg_ref[2:3, :] = ends[1]
    msg_ref[3:4, :] = ends[0]
    msg_ref[4:8, :] = jnp.zeros((4, channels), F32)
    totals = []
    for d in range(n - 1, 0, -1):
        copy = remote(msg_ref, all_ref.at[sp], s_tot, (d,), (partner_at(sp, n, d), tp))
        copy.start()
        totals.append(copy)
    all_ref[sp] = msg_ref[...]
    mixes, pairs = {}, {}
    for d in range(n - 1, 0, -1):
        peer = partner_at(sp, n, d)
        mixes[d] = remote(mixed_ref.at[peer, mine], mixed_all.at[d, mine], s_mix, (d,), (peer, tp))
        mixes[d].start()
    mixed_all[0] = mixed_ref[sp]
    gather_on()
    for copy in totals:
        copy.wait()
    in_ab, in_af = carries(n, all_ref, ((1, 2), (0, 3)))
    after_f = after_ref[0] + ones_ref[0] * in_af
    after_b = after_ref[1] + ones_ref[1] * in_ab
    adjoint = (carried + shifted(after_f, -1, in_af), carried + shifted(after_b, 1, in_ab))
    total = adjoint[0] * a_ref[0] + adjoint[1] * a_ref[1]
    for d in range(2):
        packed_ref[:, 2 * d * channels : (2 * d + 1) * channels] = adjoint[d] * c_ref[d]
        packed_ref[:, (2 * d + 1) * channels : (2 * d + 2) * channels] = adjoint[d] * e_ref[d]
    total = total + split_dot(packed_ref[...], maps_ref[...], COLS1)
    conv_grad_ref[...] = total.astype(BF)
    edges = edge_copies(n, conv_grad_ref, halo_ref, s_edge)
    while bits:
        gather_on()
    for d in range(n - 1, 0, -1):
        mixes[d].wait_recv()
        block = mixed_all.at[d, mine]
        pairs[d] = remote(block, block, s_pair, (d,), (sp, partner))
        pairs[d].start()
    for copy in edges:
        copy.wait()
    taps = taps_ref[...].astype(F32)
    low, high = halo_rows(halo_ref, n)
    up1 = shifted(total, -1, high[0:1])
    up2 = shifted(up1, -1, high[1:2])
    down = shifted(total, 1, low[1:2])
    result = up2 * taps[0:1] + up1 * taps[1:2] + total * taps[2:3] + down * taps[3:4]
    input_grad_ref[...] = result.astype(BF)
    for d in range(1, n):
        pairs[d].wait()
        mixes[d].wait_send()
    for got in gathers[:-1]:
        for copy in got:
            copy.wait_send()
    for copy in gathers[-1]:
        copy.wait()
    grad_out_ref[...] = lax.dot_general(
        mixed_all[...].reshape(n * length, part),
        out_all[...].reshape(n * length, channels),
        ROWS0,
        preferred_element_type=F32,
    )


def tail(args, n):
    ng, proj, decay = args[0], args[3], args[4]
    length, width = ng.shape
    channels = proj.shape[1]
    part = width // n
    dma = pltpu.SemaphoreType.DMA
    sds = jax.ShapeDtypeStruct
    vm = pltpu.VMEM
    two = (2, length, channels)
    return pl.pallas_call(
        functools.partial(tail_kernel, n),
        out_shape=(
            sds((part, channels), F32), sds((length, channels), BF), sds((length, channels), BF),
        ),
        in_specs=[VM] * len(args),
        out_specs=[VM] * 3,
        scratch_shapes=[
            vm((n, length, part), BF), vm((n, length, part), BF), vm((n, length, channels), BF),
            vm(two, F32), vm(two, F32), vm((8, channels), F32), vm((n, 8, channels), F32),
            vm((length, 4 * channels), F32), vm((length, channels), BF),
            vm((2, ROW_TILE, channels), BF),
            dma((2, n)), dma((2, n)), dma((2, n)), dma((2, n)), dma((2, 2)),
        ],
        compiler_params=pltpu.CompilerParams(
            collective_id=2, has_side_effects=True, vmem_limit_bytes=24 * 2**20
        ),
        cost_estimate=pl.CostEstimate(
            flops=500_000_000, bytes_accessed=10_000_000, transcendentals=0
        ),
    )(*args)


def shards(
    cotangent,
    saved_input,
    routes,
    route_weight,
    gate_proj,
    up_proj,
    down_proj,
    out_proj,
    conv_input,
    gate_branch,
    conv_taps,
    recur_map,
    input_map,
    decay_param,
    decay_shift,
):
    length, _ = cotangent.shape
    n = lax.axis_size("sp")
    n_tp = lax.axis_size("tp")
    slots = 4 * length // n
    slots = (slots + ROW_TILE - 1) // ROW_TILE * ROW_TILE
    plus = jax.nn.softplus(-decay_param)
    (
        normed_grad, grad_gate, grad_up, grad_down,
        maps, decay, ones, coef_a, coef_c, coef_e, value, slope, mixed_out, tot,
    ) = front(
        (
            cotangent, saved_input, routes.T, route_weight.T, gate_proj[0], up_proj[0], down_proj[0],
            conv_input, gate_branch, conv_taps, recur_map, input_map, decay_shift,
        ),
        plus, None, n, n_tp, slots,
    )
    grad_out, input_grad, branch_grad = tail(
        (
            normed_grad, cotangent, saved_input, out_proj, decay, ones, coef_a, coef_c, coef_e,
            value, slope, maps, tot, mixed_out, conv_taps,
        ),
        n,
    )
    return (grad_gate[None], grad_up[None], grad_down[None], grad_out, input_grad, branch_grad)


def solution(mesh):
    in_specs = (
        P("sp", None),
        P("sp", None),
        P("sp", None),
        P("sp", None),
        P("sp", None, "tp"),
        P("sp", None, "tp"),
        P("sp", "tp", None),
        P(None, "tp"),
        P("sp", "tp"),
        P("sp", "tp"),
        P(None, "tp"),
        P(None, "tp", None, None),
        P(None, "tp", None, None),
        P(None, "tp"),
        P(None, "sp", "tp"),
    )
    out_specs = (
        P("sp", None, "tp"),
        P("sp", None, "tp"),
        P("sp", "tp", None),
        P("sp", "tp"),
        P("sp", "tp"),
        P("sp", "tp"),
    )
    return jax.shard_map(shards, mesh=mesh, in_specs=in_specs, out_specs=out_specs, check_vma=False)
```

time: 153 us -> 131 us (0.86)
  Pallas kernels: 127 us -> 110 us
  matrix products: 12.8 us -> 0 us
  local copies, waits for them, and re-layouts: 8.01 us -> 19.4 us
  other arithmetic: 3.41 us -> 0.7 us
    pallas_call x8 -> x2, Pallas kernels: 127 us -> 110 us  [the longest x1 85.4 us: front(): pl.pallas_call(functools.partial(front_kernel, n, slots), out_shape=outs,...]
    dot_general x9 -> x0, matrix products: 12.8 us -> none  [the longest x1 2.35 us: shards(): lax.dot_general(hidden, rows_scaled, rows0, preferred_element_type=F32)]
    unnamed x37 -> x36, local copies, waits for them, and re-layouts: 7.12 us -> 19.4 us
where the time goes in v1:
time: 131 us
  Pallas kernels  110 us (84%)
  local copies, waits for them, and re-layouts  19.4 us (15%)
    pallas_call x1, Pallas kernels, front(): pl.pallas_call(functools.partial(front_kernel, n, slots), out_shape=outs,...  85.4 us
    pallas_call x1, Pallas kernels, tail(): pl.pallas_call(functools.partial(tail_kernel, n), out_shape=(sds((part, c...  24.6 us
    unnamed x36, local copies, waits for them, and re-layouts  19.4 us

profile of v1, /device:TPU:0, one launch (start us, length us, event | category | flops | bytes accessed | tf_op | source)
XLA Modules:
  0.0 130.8 jit_solution(18154328038214198305)
XLA Ops:
  0.6 0.7 compare_select_fusion.refs_12_
  1.3 0.0 copy-start.1
  1.3 1.1 copy-done.1
  2.4 0.0 copy-start.2
  2.4 1.1 copy-done.2
  3.5 0.0 copy-start.3
  3.5 0.7 copy-done.3
  4.2 0.0 copy-start.4
  4.2 1.2 copy-done.4
  5.4 0.0 copy-start.5
  5.4 1.2 copy-done.5
  6.6 0.0 copy-start.6
  6.6 1.2 copy-done.6
  7.9 0.0 copy-start.7
  7.9 1.0 copy-done.7
  8.8 0.0 copy-start.8
  8.8 0.9 copy-done.8
  9.7 0.0 copy-start.9
  9.7 0.9 copy-done.9
  10.7 0.0 copy-start.10
  10.7 0.9 copy-done.10
  11.5 0.0 copy-start.11
  11.5 0.9 copy-done.11
  12.4 0.0 copy-start.12
  12.4 0.7 copy-done.12
  13.1 0.0 copy-start.13
  13.1 0.7 copy-done.13
  13.8 0.0 copy-start
  13.8 85.4 %shard_map.190 = (bf16[160,2048]{1,0:T(8,128)(2,1)S(1)}, f32[2048,256]{1,0:T(8,128)S(1)}, f32[2048,256]{1,0:T(8,128)S(1)}, f32[256,2048]{1,0:T(8,128)}, bf16[256...) custom-call(bf16[160,2048]{1,0:T(8,128)(2,1)S(1)} %copy-done.1, ...), custom_call_target="tpu_custom_call" | custom-call | flops 2000000000 | bytes 30000000 | tf_op jit(solution)/shard_map/pallas_call | solution.py:525
  99.2 0.0 copy-done
  99.2 24.6 %shard_map.191 = (f32[256,256]{1,0:T(8,128)S(1)}, bf16[160,256]{1,0:T(8,128)(2,1)S(1)}, bf16[160,256]{1,0:T(8,128)(2,1)S(1)}) custom-call(bf16[160,2048]{1,0:T(8,128)(2,1)S(1)} %get-tuple-element.26.refs_0_, bf16[160,2048]{1,0:T(8,128)(2,1)S(1)} %copy-done.1, bf16[160,2048]{1,0:T(8,128)(2,1)S(1)} %copy-done.2, bf16[2048,256]{1,0:T(8,128)(2,1)S(1)} %copy-done, ...), custom_call_target="tpu_custom_call" | custom-call | flops 500000000 | bytes 10000000 | tf_op jit(solution)/shard_map/pallas_call | solution.py:688
  123.8 1.3 %copy.27 = f32[1,2048,256]{2,1,0:T(8,128)} copy(f32[1,2048,256]{2,1,0:T(8,128)S(1)} %bitcast.9) | data formatting | bytes 4194304
  125.2 0.0 copy-start.14
  125.2 1.3 %copy.28 = f32[1,2048,256]{2,1,0:T(8,128)} copy(f32[1,2048,256]{2,1,0:T(8,128)S(1)} %bitcast.8) | data formatting | bytes 4194304
  126.5 1.0 copy-done.14
  127.5 1.3 %copy.29 = f32[1,256,2048]{2,1,0:T(8,128)} copy(f32[1,256,2048]{2,1,0:T(8,128)S(1)} %bitcast.15) | data formatting | bytes 4194304
  128.8 0.7 copy.30
  129.5 0.6 copy.31
  130.2 0.6 copy.32
Async XLA Ops:
  1.3 1.1 copy-start.1
  2.4 1.1 copy-start.2
  3.5 0.7 copy-start.3
  4.2 1.2 copy-start.4
  5.4 1.2 copy-start.5
  6.6 1.2 copy-start.6
  7.9 1.0 copy-start.7
  8.8 0.9 copy-start.8
  9.7 0.9 copy-start.9
  10.7 0.9 copy-start.10
  11.5 0.9 copy-start.11
  12.4 0.7 copy-start.12
  13.1 0.7 copy-start.13
  13.8 85.4 %copy-start = (bf16[2048,256]{1,0:T(8,128)(2,1)S(1)}, bf16[2048,256]{1,0:T(8,128)(2,1)}, u32[]{:S(2)}) copy-start(bf16[2048,256]{1,0:T(8,128)(2,1)} %refs_3_.1) | copy-start | bytes 3145732
  125.2 2.3 %copy-start.14 = (f32[256,2048]{1,0:T(8,128)S(1)}, f32[256,2048]{1,0:T(8,128)}, u32[]{:S(2)}) copy-start(f32[256,2048]{1,0:T(8,128)} %get-tuple-element.25) | copy-start | bytes 6291460

commit v2 on v1

v2 whole, which is shorter than its diff:
```python
import functools
import jax
import jax.numpy as jnp
from jax import lax
from jax.experimental import pallas as pl
from jax.experimental.pallas import tpu as pltpu
from jax.sharding import PartitionSpec as P

EPS = 1e-06
DECAY_SCALE = 8.0
ROW_TILE = 16
LAG = 3
VMEM_LIMIT = 62 * 2**20
GELU_K = 0.7978845608028654
GELU_C = 0.044715
VM = pl.BlockSpec(memory_space=pltpu.VMEM)
HB = pl.BlockSpec(memory_space=pltpu.HBM)
BF = jnp.bfloat16
F32 = jnp.float32
ROWS0 = (((0,), (0,)), ((), ()))
COLS1 = (((1,), (1,)), ((), ()))
PLAIN = (((1,), (0,)), ((), ()))


def neighbours():
    tp = lax.axis_index("tp")
    side = tp // 2
    core = tp % 2
    return tp, side * 2 + (1 - core), (1 - side) * 2 + core, (1 - side) * 2 + (1 - core)


def partner_at(sp, n, d):
    if n & (n - 1):
        return (sp + d) % n
    bit, peer = 1, sp
    while bit < n:
        if d & bit:
            peer = peer + bit * (1 - 2 * ((sp // bit) % 2))
        bit *= 2
    return peer


def source_at(sp, n, d):
    return (sp + n - d) % n if n & (n - 1) else partner_at(sp, n, d)


def announce(n, tps):
    sp = lax.axis_index("sp")
    tp = lax.axis_index("tp")
    barrier = pltpu.get_barrier_semaphore()
    for d in range(1, n):
        pl.semaphore_signal(
            barrier, inc=1, device_id=((sp + d) % n, tp), device_id_type=pl.DeviceIdType.MESH
        )
    for other in tps:
        pl.semaphore_signal(barrier, inc=1, device_id=(sp, other), device_id_type=pl.DeviceIdType.MESH)
    return barrier, n - 1 + len(tps)


def remote(src, dst, sems, index, device):
    return pltpu.make_async_remote_copy(
        src_ref=src,
        dst_ref=dst,
        send_sem=sems.at[(0,) + index],
        recv_sem=sems.at[(1,) + index],
        device_id=device,
        device_id_type=pl.DeviceIdType.MESH,
    )


def edge_copies(n, x_ref, halo_ref, sems):
    sp = lax.axis_index("sp")
    tp = lax.axis_index("tp")
    length, tile = x_ref.shape[0], halo_ref.shape[1]
    copies = (
        remote(x_ref.at[pl.ds(length - tile, tile)], halo_ref.at[0], sems, (0,), ((sp + 1) % n, tp)),
        remote(x_ref.at[pl.ds(0, tile)], halo_ref.at[1], sems, (1,), ((sp + n - 1) % n, tp)),
    )
    for copy in copies:
        copy.start()
    return copies


def halo_rows(halo_ref, n):
    sp = lax.axis_index("sp")
    before = jnp.where(sp == 0, 0.0, halo_ref[0].astype(F32))
    after = jnp.where(sp == n - 1, 0.0, halo_ref[1].astype(F32))
    return before[before.shape[0] - 2 :], after[:2]


def split_dot(x, w, dims):
    high = x.astype(BF)
    low = (x - high.astype(F32)).astype(BF)
    total = lax.dot_general(low, w, dims, preferred_element_type=F32)
    return total + lax.dot_general(high, w, dims, preferred_element_type=F32)


def minus_expm1(y):
    series = 1.0 + y * (1.0 / 8.0)
    for k in (7.0, 6.0, 5.0, 4.0, 3.0, 2.0):
        series = 1.0 + y * (1.0 / k) * series
    return jnp.where(y > -0.25, -y * series, 1.0 - jnp.exp(y))


def softplus(x):
    u = jnp.exp(-jnp.abs(x))
    series = 1.0 / 9.0
    for k in (8.0, 7.0, 6.0, 5.0, 4.0, 3.0, 2.0, 1.0):
        series = 1.0 / k - u * series
    return jnp.maximum(x, 0.0) + jnp.where(u < 0.05, u * series, jnp.log(1.0 + u))


def shifted(x, by, edge):
    length = x.shape[0]
    row = lax.broadcasted_iota(jnp.int32, x.shape, 0)
    moved = pltpu.roll(x, by % length, 0)
    return jnp.where(row == (0 if by > 0 else length - 1), edge, moved)


def run_scans(length, jobs):
    width = jobs[0][1].shape[1]
    groups = length // 8

    def body(g, carry):
        out = []
        for (reverse, a_ref, b_ref, to_ref), state in zip(jobs, carry):
            base = pl.multiple_of((groups - 1 - g if reverse else g) * 8, 8)
            a = a_ref[pl.ds(base, 8), :]
            b = None if b_ref is None else b_ref[pl.ds(base, 8), :]
            rows = [None] * 8
            for k in reversed(range(8)) if reverse else range(8):
                state = a[k : k + 1] * state
                if b is not None:
                    state = state + b[k : k + 1]
                rows[k] = state
            to_ref[pl.ds(base, 8), :] = jnp.concatenate(rows, axis=0)
            out.append(state)
        return tuple(out)

    start = tuple(
        jnp.full((1, width), 1.0 if b_ref is None else 0.0, F32) for _, _, b_ref, _ in jobs
    )
    return lax.fori_loop(0, groups, body, start)


def gelu_parts(x):
    t = jnp.tanh(GELU_K * (x + GELU_C * x * x * x))
    value = 0.5 * x * (1.0 + t)
    slope = 0.5 * (1.0 + t) + 0.5 * x * (1.0 - t * t) * GELU_K * (1.0 + 3.0 * GELU_C * x * x)
    return value, slope


def carries(n, all_ref, rows):
    sp = lax.axis_index("sp")
    zero = jnp.zeros((1, all_ref.shape[2]), F32)
    (lp, le), (up, ue) = rows

    def lower(k, carry):
        t = all_ref[k]
        return t[lp : lp + 1] * carry + t[le : le + 1]

    def upper(i, carry):
        t = all_ref[n - 1 - i]
        return t[up : up + 1] * carry + t[ue : ue + 1]

    return lax.fori_loop(0, sp, lower, zero), lax.fori_loop(0, n - 1 - sp, upper, zero)


def whole_kernel(n, slots, *refs):
    (
        cot_hbm, x_hbm, routes_hbm, weight_hbm, wg_hbm, wu_hbm, wd_hbm, proj_hbm, cin_hbm,
        branch_hbm, taps_hbm, rmap_hbm, imap_hbm, param_hbm, shift_hbm,
        ggate_hbm, gup_hbm, gdown_hbm, grad_out_hbm, input_grad_hbm, branch_grad_hbm,
        routes_ref, weight_ref, cin_ref, branch_ref, taps_ref, rmap_ref, imap_ref, param_ref,
        cot_ref, x_ref, nx_ref, wg_ref, wu_ref, wd_ref, proj_ref, shift_ref,
        ng_ref, ggate_ref, gup_ref, gdown_ref, grad_out_ref, input_grad_ref, branch_grad_ref,
        pick_ref, send_ref, rows_sc, rows_in, hid_ref, ggu_ref, part_ref,
        got1, got2, mid, fin, back, halo_ref,
        maps_ref, decay_ref, ones_ref, a_ref, c_ref, e_ref, value_ref, slope_ref, tot_ref,
        conv_ref, gates_ref, root_ref, drive_ref, state_ref, cum_ref, all_ref,
        mixed_ref, mixed_all, out_all, after_ref, msg_ref, every_ref, conv_grad_ref, halo2_ref,
        loc, put, edge, hop, pair, cross, fwd, s_pair, s_cross, s_hop, s_tail, s_tot,
        s_msg, s_mix, s_share, s_out, s_edge,
    ) = refs
    length, width = cot_ref.shape
    fourth = send_ref.shape[3]
    channels = cin_ref.shape[1]
    sp = lax.axis_index("sp")
    tp, partner, across, diagonal = neighbours()
    unit = n // 8
    rows = (rows_sc, rows_in)

    def cols(q):
        return pl.ds(pl.multiple_of(q * fourth, 128), fourth)

    loads = [
        pltpu.make_async_copy(src, dst, loc.at[i])
        for i, (src, dst) in enumerate(
            (
                (x_hbm, x_ref), (cot_hbm, cot_ref), (shift_hbm, shift_ref),
                (wg_hbm, wg_ref), (wu_hbm, wu_ref), (wd_hbm, wd_ref), (proj_hbm, proj_ref),
                (cin_hbm, cin_ref), (routes_hbm, routes_ref), (weight_hbm, weight_ref),
                (taps_hbm, taps_ref), (rmap_hbm, rmap_ref), (imap_hbm, imap_ref),
                (param_hbm, param_ref), (branch_hbm, branch_ref),
            )
        )
    ]
    for i in (8, 9, 0, 1, 7, 10, 11, 12, 13, 2, 14, 3, 4, 5, 6):
        loads[i].start()

    barrier, heard = announce(n, (partner, across))
    puts = []

    def store(src, dst):
        copy = pltpu.make_async_copy(src, dst, put.at[len(puts)])
        copy.start()
        puts.append(copy)

    loads[8].wait()
    loads[9].wait()
    route0, route1 = routes_ref[0:1], routes_ref[1:2]
    offset = lax.broadcasted_iota(jnp.int32, (n, length), 0)
    which = (offset + sp) % n if n & (n - 1) else offset ^ sp
    first, second = which == route0, which == route1
    named = (first | second).astype(F32).astype(BF)
    earlier = lax.broadcasted_iota(jnp.int32, (length, length), 0) < lax.broadcasted_iota(
        jnp.int32, (length, length), 1
    )
    rank = jnp.dot(named, earlier.astype(F32).astype(BF), preferred_element_type=F32)
    place = (offset * slots).astype(F32) + rank
    target0 = jnp.sum(jnp.where(first, place, 0.0), axis=0, keepdims=True).astype(jnp.int32)
    target1 = jnp.sum(jnp.where(second, place, 0.0), axis=0, keepdims=True).astype(jnp.int32)
    loads[0].wait()
    for r in range(0, length, 32):
        x = x_ref[r : r + 32].astype(F32)
        inv = lax.rsqrt(jnp.mean(x * x, axis=1, keepdims=True) + EPS)
        nx_ref[r : r + 32] = (x * inv).astype(BF)

    def chosen(lo, hi):
        slot = lax.broadcasted_iota(jnp.int32, ((hi - lo) * slots, length), 0) + lo * slots
        hit0, hit1 = slot == target0, slot == target1
        pick = (hit0 | hit1).astype(F32).astype(BF)
        pick_ref[lo * slots : hi * slots] = pick
        share = jnp.where(hit0, weight_ref[0:1], 0.0) + jnp.where(hit1, weight_ref[1:2], 0.0)
        return pick, jnp.sum(share, axis=1, keepdims=True)

    def taken(pick, share, where):
        cot = jnp.dot(pick, cot_ref[:, where], preferred_element_type=F32)
        got = jnp.dot(pick, nx_ref[:, where], preferred_element_type=F32).astype(BF)
        return (cot * share).astype(BF), got

    order = [
        d for lo, hi in ((1, 4 * unit), (6 * unit, n), (4 * unit, 6 * unit)) for d in range(lo, hi)
    ]
    hops = {}
    loads[1].wait()
    for lo, hi in ((0, 4 * unit), (4 * unit, n)):
        pick, share = chosen(lo, hi)
        for a, value in enumerate(taken(pick, share, cols(tp))):
            send_ref[a, lo:hi] = value.reshape(hi - lo, slots, fourth)
        if lo == 0:
            own = pick[:slots], share[:slots]
            pl.semaphore_wait(barrier, heard)
            loads[7].wait()
            edges = edge_copies(n, cin_ref, halo_ref, edge)
        for d in order:
            if lo <= d < hi:
                for a in range(2):
                    copy = remote(
                        send_ref.at[a, d], rows[a].at[d, :, cols(tp)], hop, (a, d),
                        (partner_at(sp, n, d), tp),
                    )
                    copy.start()
                    hops[a, d] = copy
    for q in range(width // fourth):
        where = pl.ds(q * fourth, fourth)
        rows_sc[0, :, where], rows_in[0, :, where] = taken(*own, where)

    for i in (10, 11, 12, 13):
        loads[i].wait()
    plus = softplus(-param_ref[...])
    heads, hw = rmap_ref.shape[1], rmap_ref.shape[2]
    spread = (
        lax.broadcasted_iota(jnp.int32, (hw, channels), 1) % hw
        == lax.broadcasted_iota(jnp.int32, (hw, channels), 0)
    ).astype(F32).astype(BF)
    block = (
        lax.broadcasted_iota(jnp.int32, (channels, channels), 0) // hw
        == lax.broadcasted_iota(jnp.int32, (channels, channels), 1) // hw
    )
    for i in range(4):
        stack = (rmap_ref, imap_ref)[i % 2][i // 2].reshape(heads * hw, hw)
        full = jnp.dot(stack, spread, preferred_element_type=F32)
        maps_ref[:, i * channels : (i + 1) * channels] = jnp.where(block, full, 0.0).astype(BF)
    for copy in edges:
        copy.wait()
    taps = taps_ref[...].astype(F32)
    low, high = halo_rows(halo_ref, n)
    x = cin_ref[...].astype(F32)
    back1 = shifted(x, 1, low[1:2])
    back2 = shifted(back1, 1, low[0:1])
    conv = back2 * taps[0:1] + back1 * taps[1:2] + x * taps[2:3]
    conv = conv + shifted(x, -1, high[0:1]) * taps[3:4]
    conv_ref[...] = conv
    gates_ref[...] = jax.nn.sigmoid(split_dot(conv, maps_ref[...], PLAIN))
    loads[2].wait()
    for d in range(2):
        recur = gates_ref[:, 2 * d * channels : (2 * d + 1) * channels]
        inputs = gates_ref[:, (2 * d + 1) * channels : (2 * d + 2) * channels]
        log_decay = -DECAY_SCALE * recur * plus[d : d + 1] + shift_ref[d]
        root = jnp.sqrt(minus_expm1(2.0 * log_decay))
        decay_ref[d] = jnp.exp(log_decay)
        root_ref[d] = root
        drive_ref[d] = root * (inputs * conv_ref[...])
    a_f, a_b = decay_ref.at[0], decay_ref.at[1]
    ends = run_scans(
        length,
        (
            (False, a_f, drive_ref.at[0], state_ref.at[0]),
            (True, a_b, drive_ref.at[1], state_ref.at[1]),
            (False, a_f, None, cum_ref.at[0]),
            (True, a_b, None, cum_ref.at[1]),
            (True, a_f, None, ones_ref.at[0]),
            (False, a_b, None, ones_ref.at[1]),
        ),
    )
    tot_ref[0:1, :] = ends[2]
    tot_ref[1:2, :] = ends[0]
    tot_ref[2:3, :] = ends[3]
    tot_ref[3:4, :] = ends[1]
    tot_ref[4:8, :] = jnp.zeros((4, channels), F32)
    totals = []
    for d in range(n - 1, 0, -1):
        copy = remote(tot_ref, all_ref.at[sp], s_tot, (d,), (partner_at(sp, n, d), tp))
        copy.start()
        totals.append(copy)
    all_ref[sp] = tot_ref[...]

    def finish_states():
        for copy in totals:
            copy.wait()
        in_f, in_b = carries(n, all_ref, ((0, 1), (2, 3)))
        state_f = state_ref[0] + cum_ref[0] * in_f
        state_b = state_ref[1] + cum_ref[1] * in_b
        beside = (shifted(state_f, 1, in_f), shifted(state_b, -1, in_b))
        loads[14].wait()
        value, slope = gelu_parts(branch_ref[...].astype(F32))
        states = state_f + state_b
        value_ref[...] = value
        slope_ref[...] = states * slope
        out_all[0] = (value * states).astype(BF)
        conv = conv_ref[...]
        for d in range(2):
            recur = gates_ref[:, 2 * d * channels : (2 * d + 1) * channels]
            inputs = gates_ref[:, (2 * d + 1) * channels : (2 * d + 2) * channels]
            decay = decay_ref[d]
            root = root_ref[d]
            a_ref[d] = root * inputs
            g_log = beside[d] * decay - inputs * conv * (decay * decay) / root
            c_ref[d] = g_log * (-DECAY_SCALE * plus[d : d + 1]) * recur * (1.0 - recur)
            e_ref[d] = root * conv * inputs * (1.0 - inputs)

    nears, fwds, overs, late = {}, {}, {}, []

    def step_in(a, d):
        hops[a, d].wait_recv()
        dst = rows[a]
        mine = dst.at[d, :, cols(tp)]
        overs[a, d] = remote(mine, mine, cross, (a, d), (sp, across))
        overs[a, d].start()
        late.append((a, d))
        nears[a, d] = remote(mine, mine, pair, (a, d), (sp, partner))
        nears[a, d].start()

    def step_on():
        a, d = late.pop(0)
        overs[a, d].wait_recv()
        other = rows[a].at[d, :, cols(across)]
        fwds[a, d] = remote(other, other, fwd, (a, d), (sp, partner))
        fwds[a, d].start()

    def bring(lo, hi):
        for d in order:
            if lo * unit <= d < hi * unit:
                for a in range(2):
                    step_in(a, d)
                    if len(late) > LAG:
                        step_on()

    pairs, crosses, backs = {}, {}, {}

    def experts(lo, hi):
        lo, hi = lo * unit, hi * unit
        while any(lo <= d < hi for _, d in late):
            step_on()
        for d in range(lo, hi):
            if d:
                for a in range(2):
                    nears[a, d].wait_recv()
                    fwds[a, d].wait_recv()
        count = (hi - lo) * slots
        at = slice(lo * slots, hi * slots)
        xin = rows_in[lo:hi].reshape(count, width)
        gate_pre = jnp.dot(xin, wg_ref[...], preferred_element_type=F32)
        up_pre = jnp.dot(xin, wu_ref[...], preferred_element_type=F32)
        xsc = rows_sc[lo:hi].reshape(count, width)
        hidden_grad = lax.dot_general(xsc, wd_ref[...], COLS1, preferred_element_type=F32)
        gate_sig = jax.nn.sigmoid(gate_pre)
        gate_act = gate_pre * gate_sig
        hid_ref[at] = (gate_act * up_pre).astype(BF)
        gate_grad = hidden_grad * up_pre * gate_sig * (1.0 + gate_pre * (1.0 - gate_sig))
        gate_grad = gate_grad.astype(BF)
        up_grad = (hidden_grad * gate_act).astype(BF)
        units = up_grad.shape[1]
        ggu_ref[at, :units] = gate_grad
        ggu_ref[at, units:] = up_grad
        for i, q in enumerate((diagonal, partner, across, tp)):
            some = pl.ds(pl.multiple_of(q * fourth, 128), fourth)
            total = lax.dot_general(gate_grad, wg_ref[some], COLS1, preferred_element_type=F32)
            total = total + lax.dot_general(up_grad, wu_ref[some], COLS1, preferred_element_type=F32)
            part_ref[lo:hi, :, cols(q)] = total.astype(BF).reshape(hi - lo, slots, fourth)
            if i < 2:
                for d in range(lo, hi):
                    copy = remote(
                        part_ref.at[d, :, cols(q)], got1.at[i, d], s_pair, (i, d), (sp, partner)
                    )
                    copy.start()
                    pairs[i, d] = copy

    def stage_b(lo, hi):
        for d in range(lo * unit, hi * unit):
            pairs[0, d].wait_recv()
            total = part_ref[d, :, cols(across)].astype(F32) + got1[0, d].astype(F32)
            mid[d] = total.astype(BF)
            crosses[d] = remote(mid.at[d], got2.at[d], s_cross, (d,), (sp, across))
            crosses[d].start()

    def stage_c(lo, hi):
        for d in range(lo * unit, hi * unit):
            pairs[1, d].wait_recv()
            crosses[d].wait_recv()
            total = part_ref[d, :, cols(tp)].astype(F32) + got1[1, d].astype(F32)
            total = (total + got2[d].astype(F32)).astype(BF)
            if d == 0:
                back[0] = total
            else:
                fin[d] = total
                backs[d] = remote(fin.at[d], back.at[d], s_hop, (d,), (source_at(sp, n, d), tp))
                backs[d].start()

    chunk = width // 8

    def weight_gradients(k):
        at = slice(k * chunk, (k + 1) * chunk)
        units = hid_ref.shape[1]
        left = rows_in[:, :, at].reshape(n * slots, chunk)
        both = lax.dot_general(left, ggu_ref[...], ROWS0, preferred_element_type=F32)
        ggate_ref[at] = both[:, :units]
        gup_ref[at] = both[:, units:]
        right = rows_sc[:, :, at].reshape(n * slots, chunk)
        gdown_ref[:, at] = lax.dot_general(hid_ref[...], right, ROWS0, preferred_element_type=F32)
        store(ggate_ref.at[at], ggate_hbm.at[at])
        store(gup_ref.at[at], gup_hbm.at[at])
        store(gdown_ref.at[:, at], gdown_hbm.at[:, at])

    powers = n & (n - 1) == 0
    bits = [n >> i for i in range(1, n.bit_length())] if powers else []
    gathers = []

    def gather(pairs_of):
        got = []
        for d, to, hop_to in pairs_of:
            copy = remote(out_all.at[d], out_all.at[to], s_out, (to,), (partner_at(sp, n, hop_to), tp))
            copy.start()
            got.append(copy)
        gathers.append(got)

    def gather_start():
        if powers:
            bit = bits.pop(0)
            gather([(d, d + bit, bit) for d in range(0, n, 2 * bit)])
        else:
            gather([(0, d, d) for d in range(1, n)])

    def gather_on():
        if bits:
            for copy in gathers[-1]:
                copy.wait_recv()
            gather_start()

    bring(0, 2)
    bring(2, 4)
    for i in (3, 4, 5):
        loads[i].wait()
    experts(0, 2)
    bring(6, 8)
    experts(2, 4)
    bring(4, 6)
    experts(6, 8)
    stage_b(6, 8)
    experts(4, 6)
    stage_c(6, 8)
    stage_b(4, 6)
    stage_b(2, 4)
    stage_c(4, 6)
    stage_b(0, 2)
    stage_c(2, 4)
    stage_c(0, 2)
    finish_states()
    weight_gradients(0)
    gather_start()
    for k in range(1, 8):
        weight_gradients(k)
    for d in range(1, n):
        backs[d].wait_recv()
    got = back[...].reshape(n * slots, fourth)
    grad = lax.dot_general(pick_ref[...], got, ROWS0, preferred_element_type=F32)
    ng_ref[:, cols(tp)] = grad.astype(BF)
    own = ng_ref.at[:, cols(tp)]
    over = remote(own, own, s_tail, (0,), (sp, across))
    near = remote(own, own, s_tail, (1,), (sp, partner))
    over.start()
    near.start()
    over.wait_recv()
    other = ng_ref.at[:, cols(across)]
    last = remote(other, other, s_tail, (2,), (sp, partner))
    last.start()
    gather_on()
    for group in (hops, nears, fwds, overs, pairs, crosses, backs):
        for copy in group.values():
            copy.wait_send()
    near.wait()
    over.wait_send()
    last.wait()

    part = width // n
    half = length // 2
    mine = pl.ds(pl.multiple_of((tp % 2) * half, ROW_TILE), half)
    for r in range(0, length, 32):
        x = x_ref[r : r + 32].astype(F32)
        inv = lax.rsqrt(jnp.mean(x * x, axis=1, keepdims=True) + EPS)
        normed = x * inv
        ng = ng_ref[r : r + 32].astype(F32)
        dot = jnp.mean(ng * normed, axis=1, keepdims=True)
        mixed = (cot_ref[r : r + 32].astype(F32) + inv * (ng - normed * dot)).astype(BF)
        for e in range(n):
            mixed_ref[e, r : r + 32] = mixed[:, e * part : (e + 1) * part]
    mixes, shares = {}, {}

    def mix(ds):
        for d in ds:
            peer = partner_at(sp, n, d)
            mixes[d] = remote(
                mixed_ref.at[peer, mine], mixed_all.at[d, mine], s_mix, (d,), (peer, tp)
            )
            mixes[d].start()

    reach = order[::-1]
    early = reach[: 2 * unit]
    mix(early)
    loads[6].wait()
    out_grad = jnp.zeros((length, channels), F32)
    for e in range(n):
        out_grad = out_grad + jnp.dot(
            mixed_ref[e], proj_ref[e * part : (e + 1) * part], preferred_element_type=F32
        )
    carried = out_grad * value_ref[...]
    branch_grad_ref[...] = (out_grad * slope_ref[...]).astype(BF)
    store(branch_grad_ref, branch_grad_hbm)
    drive_ref[...] = decay_ref[...] * carried[None]
    ends = run_scans(
        length,
        (
            (True, decay_ref.at[0], drive_ref.at[0], after_ref.at[0]),
            (False, decay_ref.at[1], drive_ref.at[1], after_ref.at[1]),
        ),
    )
    msg_ref[0:1, :] = tot_ref[0:1, :]
    msg_ref[1:2, :] = tot_ref[2:3, :]
    msg_ref[2:3, :] = ends[1]
    msg_ref[3:4, :] = ends[0]
    msg_ref[4:8, :] = jnp.zeros((4, channels), F32)
    sums = []
    for d in range(n - 1, 0, -1):
        copy = remote(msg_ref, every_ref.at[sp], s_msg, (d,), (partner_at(sp, n, d), tp))
        copy.start()
        sums.append(copy)
    every_ref[sp] = msg_ref[...]
    mix([d for d in reach if d not in early])
    mixed_all[0] = mixed_ref[sp]
    gather_on()
    for copy in sums:
        copy.wait()
    in_ab, in_af = carries(n, every_ref, ((1, 2), (0, 3)))
    after_f = after_ref[0] + ones_ref[0] * in_af
    after_b = after_ref[1] + ones_ref[1] * in_ab
    adjoint = (carried + shifted(after_f, -1, in_af), carried + shifted(after_b, 1, in_ab))
    total = adjoint[0] * a_ref[0] + adjoint[1] * a_ref[1]
    for d in range(2):
        gates_ref[:, 2 * d * channels : (2 * d + 1) * channels] = adjoint[d] * c_ref[d]
        gates_ref[:, (2 * d + 1) * channels : (2 * d + 2) * channels] = adjoint[d] * e_ref[d]
    total = total + split_dot(gates_ref[...], maps_ref[...], COLS1)
    conv_grad_ref[...] = total.astype(BF)
    rims = edge_copies(n, conv_grad_ref, halo2_ref, s_edge)
    while bits:
        gather_on()
    for d in reach:
        mixes[d].wait_recv()
        block = mixed_all.at[d, mine]
        shares[d] = remote(block, block, s_share, (d,), (sp, partner))
        shares[d].start()
    for copy in rims:
        copy.wait()
    taps = taps_ref[...].astype(F32)
    low, high = halo_rows(halo2_ref, n)
    up1 = shifted(total, -1, high[0:1])
    up2 = shifted(up1, -1, high[1:2])
    down = shifted(total, 1, low[1:2])
    result = up2 * taps[0:1] + up1 * taps[1:2] + total * taps[2:3] + down * taps[3:4]
    input_grad_ref[...] = result.astype(BF)
    store(input_grad_ref, input_grad_hbm)
    for d in range(1, n):
        shares[d].wait()
        mixes[d].wait_send()
    for got in gathers[:-1]:
        for copy in got:
            copy.wait_send()
    for copy in gathers[-1]:
        copy.wait()
    grad_out_ref[...] = lax.dot_general(
        mixed_all[...].reshape(n * length, part),
        out_all[...].reshape(n * length, channels),
        ROWS0,
        preferred_element_type=F32,
    )
    store(grad_out_ref, grad_out_hbm)
    for copy in puts:
        copy.wait()


def whole(args, n, n_tp, slots):
    cot, wg, proj, cin = args[0], args[4], args[7], args[8]
    length, width = cot.shape
    channels = cin.shape[1]
    units = wg.shape[1]
    fourth = width // n_tp
    part = width // n
    dma = pltpu.SemaphoreType.DMA
    sds = jax.ShapeDtypeStruct
    vm = pltpu.VMEM
    one, two = (length, channels), (2, length, channels)
    outs = (
        sds((width, units), F32),
        sds((width, units), F32),
        sds((units, width), F32),
        sds((part, channels), F32),
        sds(one, BF),
        sds(one, BF),
    )
    block = (n, slots, fourth)
    scratch = [
        *(vm(args[i].shape, args[i].dtype) for i in (2, 3, 8, 9, 10, 11, 12, 13)),
        vm((length, width), BF), vm((length, width), BF), vm((length, width), BF),
        vm((width, units), BF), vm((width, units), BF), vm((units, width), BF),
        vm(proj.shape, BF), vm(two, F32),
        vm((length, width), BF),
        *(vm(out.shape, out.dtype) for out in outs),
        vm((n * slots, length), BF), vm((2,) + block, BF),
        vm((n, slots, width), BF), vm((n, slots, width), BF),
        vm((n * slots, units), BF), vm((n * slots, 2 * units), BF), vm((n, slots, width), BF),
        vm((2,) + block, BF), vm(block, BF), vm(block, BF), vm(block, BF), vm(block, BF),
        vm((2, ROW_TILE, channels), BF),
        vm((channels, 4 * channels), BF),
        vm(two, F32), vm(two, F32), vm(two, F32), vm(two, F32), vm(two, F32),
        vm(one, F32), vm(one, F32), vm((8, channels), F32),
        vm(one, F32), vm((length, 4 * channels), F32), vm(two, F32), vm(two, F32), vm(two, F32),
        vm(two, F32), vm((n, 8, channels), F32),
        vm((n, length, part), BF), vm((n, length, part), BF), vm((n, length, channels), BF),
        vm(two, F32), vm((8, channels), F32), vm((n, 8, channels), F32),
        vm((length, channels), BF), vm((2, ROW_TILE, channels), BF),
        dma((15,)), dma((3 * 8 + 3,)),
        dma((2, 2)), dma((2, 2, n)), dma((2, 2, n)), dma((2, 2, n)),
        dma((2, 2, n)), dma((2, 2, n)), dma((2, n)), dma((2, n)), dma((2, 3)), dma((2, n)),
        dma((2, n)), dma((2, n)), dma((2, n)), dma((2, n)), dma((2, 2)),
    ]
    return pl.pallas_call(
        functools.partial(whole_kernel, n, slots),
        out_shape=outs,
        in_specs=[HB] * len(args),
        out_specs=[HB] * len(outs),
        scratch_shapes=scratch,
        compiler_params=pltpu.CompilerParams(
            collective_id=1, has_side_effects=True, vmem_limit_bytes=VMEM_LIMIT
        ),
        cost_estimate=pl.CostEstimate(
            flops=2_000_000_000, bytes_accessed=30_000_000, transcendentals=0
        ),
    )(*args)


def written(*arrays):
    count = len(arrays)
    cuts = [8 if x.size * x.dtype.itemsize > 2**20 else 1 for x in arrays]
    offsets = [sum(cuts[:i]) for i in range(count)]

    def kernel(*refs):
        sems = refs[-1]
        sets = []
        for i in range(count):
            src, dst, held = refs[i], refs[count + i], refs[2 * count + i]
            step = src.shape[0] // cuts[i]
            for k in range(cuts[i]):
                at = pl.ds(k * step, step)
                j = offsets[i] + k
                inward = pltpu.make_async_copy(src.at[at], held.at[at], sems.at[0, j])
                outward = pltpu.make_async_copy(held.at[at], dst.at[at], sems.at[1, j])
                inward.start()
                sets.append((inward, outward))
        for inward, outward in sets:
            inward.wait()
            outward.start()
        for _, outward in sets:
            outward.wait()

    return pl.pallas_call(
        kernel,
        out_shape=tuple(jax.ShapeDtypeStruct(x.shape, x.dtype) for x in arrays),
        in_specs=[HB] * count,
        out_specs=[HB] * count,
        scratch_shapes=[pltpu.VMEM(x.shape, x.dtype) for x in arrays]
        + [pltpu.SemaphoreType.DMA((2, sum(cuts)))],
        compiler_params=pltpu.CompilerParams(vmem_limit_bytes=VMEM_LIMIT),
    )(*arrays)


def shards(
    cotangent,
    saved_input,
    routes,
    route_weight,
    gate_proj,
    up_proj,
    down_proj,
    out_proj,
    conv_input,
    gate_branch,
    conv_taps,
    recur_map,
    input_map,
    decay_param,
    decay_shift,
):
    length, _ = cotangent.shape
    n = lax.axis_size("sp")
    n_tp = lax.axis_size("tp")
    slots = 4 * length // n
    slots = (slots + ROW_TILE - 1) // ROW_TILE * ROW_TILE
    grad_gate, grad_up, grad_down, *others = written(
        *whole(
            (
                cotangent, saved_input, routes.T, route_weight.T, gate_proj[0], up_proj[0],
                down_proj[0], out_proj, conv_input, gate_branch, conv_taps, recur_map, input_map,
                decay_param, decay_shift,
            ),
            n, n_tp, slots,
        )
    )
    return (grad_gate[None], grad_up[None], grad_down[None], *others)


def solution(mesh):
    in_specs = (
        P("sp", None),
        P("sp", None),
        P("sp", None),
        P("sp", None),
        P("sp", None, "tp"),
        P("sp", None, "tp"),
        P("sp", "tp", None),
        P(None, "tp"),
        P("sp", "tp"),
        P("sp", "tp"),
        P(None, "tp"),
        P(None, "tp", None, None),
        P(None, "tp", None, None),
        P(None, "tp"),
        P(None, "sp", "tp"),
    )
    out_specs = (
        P("sp", None, "tp"),
        P("sp", None, "tp"),
        P("sp", "tp", None),
        P("sp", "tp"),
        P("sp", "tp"),
        P("sp", "tp"),
    )
    return jax.shard_map(shards, mesh=mesh, in_specs=in_specs, out_specs=out_specs, check_vma=False)
```

time: 131 us -> 95.4 us (0.73)
  local copies, waits for them, and re-layouts: 19.4 us -> 0 us
  Pallas kernels: 110 us -> 94.5 us
    unnamed x36 -> x0, local copies, waits for them, and re-layouts: 19.4 us -> none
    pallas_call x2, Pallas kernels: 110 us -> 94.5 us  [the longest x1 88.7 us: whole(): pl.pallas_call(functools.partial(whole_kernel, n, slots), out_shape=outs,...]
where the time goes in v2:
time: 95.4 us; the launch traced here: 95.3 us
  Pallas kernels  94.5 us (99%)
    pallas_call x1, Pallas kernels, whole(): pl.pallas_call(functools.partial(whole_kernel, n, slots), out_shape=outs,...  88.7 us
    pallas_call x1, Pallas kernels, written(): pl.pallas_call(kernel, out_shape=tuple((jax.ShapeDtypeStruct(x.shape, x.d...  5.74 us

profile of v2, /device:TPU:0, one launch (start us, length us, event | category | flops | bytes accessed | tf_op | source)
XLA Modules:
  0.0 95.3 jit_solution(4396013313656735720)
XLA Ops:
  0.6 88.7 %shard_map.190 = (f32[2048,256]{1,0:T(8,128)}, f32[2048,256]{1,0:T(8,128)}, f32[256,2048]{1,0:T(8,128)}, f32[256,256]{1,0:T(8,128)}, bf16[160,256]{1,0:T(8,128)(2,1)}, /*index=5*/bf16[160,256]{1,0:T(8,128)(2,1)}) custom-call(bf16[160,2048]{1,0:T(8,128)(2,1)} %refs_0_.1, bf16[160,2048]{1,0:T(8,128)(2,1)} %refs_1_.1, s32[2,160]{1,0:T(2,128)} %bitcast.14, ...), custom_call_target="tpu_custom_call" | custom-call | flops 2000000000 | bytes 30000000 | tf_op jit(solution)/shard_map/pallas_call | solution.py:686
  89.4 5.7 %shard_map.191 = (f32[2048,256]{1,0:T(8,128)}, f32[2048,256]{1,0:T(8,128)}, f32[256,2048]{1,0:T(8,128)}, f32[256,256]{1,0:T(8,128)}, bf16[160,256]{1,0:T(8,128)(2,1)}, /*index=5*/bf16[160,256]{1,0:T(8,128)(2,1)}) custom-call(f32[2048,256]{1,0:T(8,128)} %get-tuple-element.18.refs_0_, f32[2048,256]{1,0:T(8,128)} %get-tuple-element.19.refs_1_, ...), custom_call_target="tpu_custom_call" | custom-call | tf_op jit(solution)/shard_map/pallas_call | solution.py:725

commit v3 on v2

--- a/solution.py
+++ b/solution.py
@@ -517,34 +517,40 @@
     grad = lax.dot_general(pick_ref[...], got, ROWS0, preferred_element_type=F32)
     ng_ref[:, cols(tp)] = grad.astype(BF)
     own = ng_ref.at[:, cols(tp)]
-    over = remote(own, own, s_tail, (0,), (sp, across))
-    near = remote(own, own, s_tail, (1,), (sp, partner))
-    over.start()
+    half = length // 2
+    overs_h, lasts = [], []
+    for h in range(2):
+        block = ng_ref.at[pl.ds(h * half, half), cols(tp)]
+        overs_h.append(remote(block, block, s_tail, (h,), (sp, across)))
+        overs_h[h].start()
+    near = remote(own, own, s_tail, (2,), (sp, partner))
     near.start()
-    over.wait_recv()
-    other = ng_ref.at[:, cols(across)]
-    last = remote(other, other, s_tail, (2,), (sp, partner))
-    last.start()
+    for h in range(2):
+        overs_h[h].wait_recv()
+        block = ng_ref.at[pl.ds(h * half, half), cols(across)]
+        lasts.append(remote(block, block, s_tail, (3 + h,), (sp, partner)))
+        lasts[h].start()
     gather_on()
     for group in (hops, nears, fwds, overs, pairs, crosses, backs):
         for copy in group.values():
             copy.wait_send()
     near.wait()
-    over.wait_send()
-    last.wait()
+    for copy in overs_h:
+        copy.wait_send()
 
     part = width // n
-    half = length // 2
     mine = pl.ds(pl.multiple_of((tp % 2) * half, ROW_TILE), half)
-    for r in range(0, length, 32):
-        x = x_ref[r : r + 32].astype(F32)
+    for r in range(0, length, ROW_TILE):
+        if r % half == 0:
+            lasts[r // half].wait()
+        x = x_ref[r : r + ROW_TILE].astype(F32)
         inv = lax.rsqrt(jnp.mean(x * x, axis=1, keepdims=True) + EPS)
         normed = x * inv
-        ng = ng_ref[r : r + 32].astype(F32)
+        ng = ng_ref[r : r + ROW_TILE].astype(F32)
         dot = jnp.mean(ng * normed, axis=1, keepdims=True)
-        mixed = (cot_ref[r : r + 32].astype(F32) + inv * (ng - normed * dot)).astype(BF)
+        mixed = (cot_ref[r : r + ROW_TILE].astype(F32) + inv * (ng - normed * dot)).astype(BF)
         for e in range(n):
-            mixed_ref[e, r : r + 32] = mixed[:, e * part : (e + 1) * part]
+            mixed_ref[e, r : r + ROW_TILE] = mixed[:, e * part : (e + 1) * part]
     mixes, shares = {}, {}
 
     def mix(ds):
@@ -556,7 +562,7 @@
             mixes[d].start()
 
     reach = order[::-1]
-    early = reach[: 2 * unit]
+    early = []
     mix(early)
     loads[6].wait()
     out_grad = jnp.zeros((length, channels), F32)
@@ -680,7 +686,7 @@
         vm((length, channels), BF), vm((2, ROW_TILE, channels), BF),
         dma((15,)), dma((3 * 8 + 3,)),
         dma((2, 2)), dma((2, 2, n)), dma((2, 2, n)), dma((2, 2, n)),
-        dma((2, 2, n)), dma((2, 2, n)), dma((2, n)), dma((2, n)), dma((2, 3)), dma((2, n)),
+        dma((2, 2, n)), dma((2, 2, n)), dma((2, n)), dma((2, n)), dma((2, 5)), dma((2, n)),
         dma((2, n)), dma((2, n)), dma((2, n)), dma((2, n)), dma((2, 2)),
     ]
     return pl.pallas_call(
@@ -700,7 +706,7 @@
 
 def written(*arrays):
     count = len(arrays)
-    cuts = [8 if x.size * x.dtype.itemsize > 2**20 else 1 for x in arrays]
+    cuts = [4 if x.size * x.dtype.itemsize > 2**20 else 1 for x in arrays]
     offsets = [sum(cuts[:i]) for i in range(count)]
 
     def kernel(*refs):

time: 95.4 us -> 95 us (level)
  no operation moved by 1% of the time
where the time goes in v3:
time: 95 us; the launch traced here: 94.8 us
  Pallas kernels  94 us (99%)
    pallas_call x1, Pallas kernels, whole(): pl.pallas_call(functools.partial(whole_kernel, n, slots), out_shape=outs,...  88.4 us
    pallas_call x1, Pallas kernels, written(): pl.pallas_call(kernel, out_shape=tuple((jax.ShapeDtypeStruct(x.shape, x.d...  5.62 us

profile of v3, /device:TPU:0, one launch (start us, length us, event | category | flops | bytes accessed | tf_op | source)
XLA Modules:
  0.0 94.8 jit_solution(355667905877623321)
XLA Ops:
  0.6 88.4 %shard_map.190 = (f32[2048,256]{1,0:T(8,128)}, f32[2048,256]{1,0:T(8,128)}, f32[256,2048]{1,0:T(8,128)}, f32[256,256]{1,0:T(8,128)}, bf16[160,256]{1,0:T(8,128)(2,1)}, /*index=5*/bf16[160,256]{1,0:T(8,128)(2,1)}) custom-call(bf16[160,2048]{1,0:T(8,128)(2,1)} %refs_0_.1, bf16[160,2048]{1,0:T(8,128)(2,1)} %refs_1_.1, s32[2,160]{1,0:T(2,128)} %bitcast.14, ...), custom_call_target="tpu_custom_call" | custom-call | flops 2000000000 | bytes 30000000 | tf_op jit(solution)/shard_map/pallas_call | solution.py:692
  89.1 5.6 %shard_map.191 = (f32[2048,256]{1,0:T(8,128)}, f32[2048,256]{1,0:T(8,128)}, f32[256,2048]{1,0:T(8,128)}, f32[256,256]{1,0:T(8,128)}, bf16[160,256]{1,0:T(8,128)(2,1)}, /*index=5*/bf16[160,256]{1,0:T(8,128)(2,1)}) custom-call(f32[2048,256]{1,0:T(8,128)} %get-tuple-element.18.refs_0_, f32[2048,256]{1,0:T(8,128)} %get-tuple-element.19.refs_1_, ...), custom_call_target="tpu_custom_call" | custom-call | tf_op jit(solution)/shard_map/pallas_call | solution.py:731
